TPU v7x, 32 devices: a whole 2x2x4 slice. The times are simulated.
32 devices in a mesh: sp: 8 (over z, y), dp: 4 (over x, core).
Axes of the slice: x: 2, y: 2, z: 4, core: 2. Of those that a mesh axis runs over, the one named last changes fastest.
Arguments:
- inputs: bfloat16 [4, 1536, 2048], P('dp', 'sp'), may hold values from -6 to 6
- in_gain: float32 [2048], replicated, may hold values from 0.1 to 1.9
- w_query: bfloat16 [2048, 1024], P('dp', 'sp'), may hold values from -0.125 to 0.125
- w_key: bfloat16 [2048, 256], P('dp', 'sp'), may hold values from -0.375 to 0.375
- w_value: bfloat16 [2048, 256], P('dp', 'sp'), may hold values from -0.125 to 0.125
- key_bias: float32 [4, 1536, 16], P('dp', None, 'sp'), may hold values from -20 to 0
- out_gain: float32 [1024], replicated, may hold values from 0.1 to 1.9
- w_out: bfloat16 [1024, 2048], P('sp', 'dp'), may hold values from -0.1875 to 0.1875
Outputs:
- mixed: bfloat16 [4, 1536, 2048], P('dp', 'sp')
All inputs are finite; a program needn't handle non-finite values.
Results may differ from a plain program's by a relative error of at most 0.012.
The roundings to bfloat16 on the way count: a program that leaves them out, or rounds other values in their place, can miss the bound.
Values may be sent and summed in bfloat16 or wider, within the bound.
A program may use at most 128 MiB of HBM per device.

v0:
```python
import functools

import jax
import jax.numpy as jnp
from jax import lax
from jax.experimental import pallas as pl
from jax.experimental.pallas import tpu as pltpu
from jax.sharding import PartitionSpec as P

HEAD_DIM = 64
MESH = pl.DeviceIdType.MESH
VMEM_SPEC = pl.BlockSpec(memory_space=pltpu.VMEM)


norm_eps = 1e-06


def greet(peers):
    barrier = pltpu.get_barrier_semaphore()
    for peer in peers:
        pl.semaphore_signal(barrier, inc=1, device_id=peer, device_id_type=MESH)
    pl.semaphore_wait(barrier, len(peers))


def remote(source, target, send, recv, peer):
    copy = pltpu.make_async_remote_copy(
        src_ref=source, dst_ref=target, send_sem=send, recv_sem=recv,
        device_id=peer, device_id_type=MESH,
    )
    copy.start()
    return copy


def project_kernel(
    zones, group, x_ref, gain_ref, piece_ref, q_ref, kv_ref,
    weights, x_far, normed, kv_parts,
    own_sem, send_z, recv_z, send_x, recv_x, send_c, recv_c, send_y, recv_y,
):
    cores = 2
    columns = lax.axis_size("dp") // cores
    sp, dp = lax.axis_index("sp"), lax.axis_index("dp")
    zone, place = sp // group, sp % group
    column, core = dp // cores, dp % cores
    rows, width = x_ref.shape
    pieces = columns * cores
    depth = width // pieces
    half = depth // 2
    cq = piece_ref.shape[1]
    ck2 = kv_parts.shape[3]

    def at_zone(k):
        return {"sp": lax.rem(zone + k, zones) * group + place}

    def at_column(j):
        return {"dp": lax.rem(column + j, columns) * cores + core}

    def at_place(g):
        return {"sp": zone * group + lax.rem(place + g, group)}

    partner = {"dp": column * cores + (1 - core)}
    greet(
        [at_zone(k) for k in range(1, zones)]
        + [at_column(j) for j in range(1, columns)]
        + [at_place(g) for g in range(1, group)]
        + [partner]
    )

    def slot(k, j, c):
        return k * pieces + j * cores + c

    sent = []
    zone_copies, column_copies, core_copies = {}, {}, {}
    own = pltpu.make_async_copy(piece_ref, weights.at[0], own_sem)
    own.start()

    def spread_own(k):
        source = piece_ref if k == 0 else weights.at[slot(k, 0, 0)]
        for j in range(1, columns):
            column_copies[k, j] = remote(
                source, weights.at[slot(k, j, 0)], send_x.at[k, j], recv_x.at[k, j], at_column(j)
            )
        core_copies[k, 0] = remote(
            source, weights.at[slot(k, 0, 1)], send_c.at[k, 0], recv_c.at[k, 0], partner
        )

    def spread_column(k):
        for j in range(1, columns):
            column_copies[k, j].wait_recv()
            core_copies[k, j] = remote(
                weights.at[slot(k, j, 0)], weights.at[slot(k, j, 1)],
                send_c.at[k, j], recv_c.at[k, j], partner,
            )

    for k in range(1, zones):
        zone_copies[k] = remote(
            piece_ref, weights.at[slot(k, 0, 0)], send_z.at[k], recv_z.at[k], at_zone(k)
        )
    spread_own(0)
    place_copies = [
        remote(x_ref, x_far.at[g], send_y.at[g], recv_y.at[g], at_place(g))
        for g in range(1, group)
    ]

    step = 16

    def normalize(source, g):
        def chunk(n, carry):
            here = pl.ds(pl.multiple_of(n * step, step), step)
            wide = source[here, :].astype(jnp.float32)
            scale = lax.rsqrt(jnp.mean(wide * wide, axis=-1, keepdims=True) + norm_eps)
            for d in range(pieces):
                j, c = d // cores, d % cores
                index = lax.rem(column - j + columns, columns) * cores + (
                    core if c == 0 else 1 - core
                )
                for s in range(2):
                    lanes = pl.ds(pl.multiple_of(index * depth + s * half, half), half)
                    part = source[here, lanes].astype(jnp.float32) * scale * gain_ref[:, lanes]
                    normed[g, s, here, d * half : (d + 1) * half] = part.astype(jnp.bfloat16)
            return carry

        lax.fori_loop(0, rows // step, chunk, 0)

    def project(k, g):
        zone_of = lax.rem(zone - k + zones, zones)
        place_of = lax.rem(place - g + group, group)
        first = k * pieces
        key_weights = weights[pl.ds(first, pieces), depth : depth + half, :]
        key_weights = key_weights.reshape(pieces * half, cq)
        both = []
        for s in range(2):
            query_weights = weights[pl.ds(first, pieces), s * half : (s + 1) * half, :]
            query_weights = query_weights.reshape(pieces * half, cq)
            both.append(
                jnp.dot(
                    normed[g, s], jnp.concatenate([query_weights, key_weights], axis=1),
                    preferred_element_type=jnp.float32,
                )
            )
        target = pl.ds(pl.multiple_of(place_of * rows, rows), rows)
        q_ref[zone_of, target, :] = (both[0][:, :cq] + both[1][:, :cq]).astype(jnp.bfloat16)
        kv_parts[zone_of, place_of] = (
            both[0][:, cq : cq + ck2] + both[1][:, cq + ck2 : cq + 2 * ck2]
        )

    def settle(k):
        for j in range(columns):
            core_copies[k, j].wait_recv()
        project(k, 0)

    normalize(x_ref, 0)
    own.wait()
    for k in range(zones):
        if k > 0:
            zone_copies[k].wait_recv()
            spread_own(k)
            spread_column(k - 1)
        if k > 1:
            settle(k - 2)
    spread_column(zones - 1)
    for k in range(max(zones - 2, 0), zones):
        settle(k)
    for g in range(1, group):
        place_copies[g - 1].wait_recv()
        normalize(x_far.at[g], g)

        def later(k, carry):
            project(k, g)
            return carry

        lax.fori_loop(0, zones, later, 0)
    for z in range(zones):
        kv_ref[z] = jnp.concatenate(
            [kv_parts[z, g] for g in range(group)], axis=1
        ).astype(jnp.bfloat16)
    for copies in (zone_copies, column_copies, core_copies):
        for copy in copies.values():
            copy.wait_send()
    for copy in place_copies:
        copy.wait_send()


def project(x, gain, piece, zones, group, ck2):
    rows, width = x.shape
    pieces = lax.axis_size("dp")
    columns = pieces // 2
    cq = piece.shape[1]
    dma = pltpu.SemaphoreType.DMA
    return pl.pallas_call(
        functools.partial(project_kernel, zones, group),
        out_shape=(
            jax.ShapeDtypeStruct((zones, group * rows, cq), jnp.bfloat16),
            jax.ShapeDtypeStruct((zones, rows, group * ck2), jnp.bfloat16),
        ),
        in_specs=[VMEM_SPEC] * 3,
        out_specs=[VMEM_SPEC] * 2,
        scratch_shapes=[
            pltpu.VMEM((zones * pieces,) + piece.shape, jnp.bfloat16),
            pltpu.VMEM((group, rows, width), jnp.bfloat16),
            pltpu.VMEM((group, 2, rows, width // 2), jnp.bfloat16),
            pltpu.VMEM((zones, group, rows, ck2), jnp.float32),
            dma,
            dma((zones,)), dma((zones,)),
            dma((zones, columns)), dma((zones, columns)),
            dma((zones, columns)), dma((zones, columns)),
            dma((group,)), dma((group,)),
        ],
        compiler_params=pltpu.CompilerParams(collective_id=0, has_side_effects=True),
        name="project",
    )(x, gain, piece)


def mixer_kernel(
    zones, group, block, q_ref, kv_ref, w_ref, bias_ref, gain_ref, out_ref,
    q_all, kv_all, k_all, v_all, w_all, head, arrived, joined,
    own_sem, send_q, recv_q, send_k, recv_k, send_z, recv_z, send_x, recv_x,
    send_y, recv_y, send_c, recv_c, send_h, recv_h,
):
    cores = 2
    size = zones * group
    columns = lax.axis_size("dp") // cores
    sp, dp = lax.axis_index("sp"), lax.axis_index("dp")
    zone, place = sp // group, sp % group
    column, core = dp // cores, dp % cores
    rows, width = out_ref.shape
    length, cq = q_all.shape
    heads = bias_ref.shape[0]
    span = group * rows
    ck = HEAD_DIM // group
    w_cols = w_ref.shape[1]

    def at(k, g):
        return {"sp": lax.rem(zone + k, zones) * group + lax.rem(place + g, group)}

    def at_column(j):
        return {"dp": lax.rem(column + j, columns) * cores + core}

    partner = {"dp": column * cores + (1 - core)}
    others = [(k, g) for k in range(zones) for g in range(group) if k + g > 0]
    greet([at(k, g) for k, g in others] + [at_column(j) for j in range(1, columns)] + [partner])

    here = pl.ds(pl.multiple_of(zone * span, span), span)
    local = [
        pltpu.make_async_copy(q_ref.at[zone], q_all.at[here, :], own_sem.at[0]),
        pltpu.make_async_copy(kv_ref.at[zone], kv_all.at[zone, place], own_sem.at[1]),
    ]
    own_lanes = pl.ds(pl.multiple_of(dp * w_cols, w_cols), w_cols)
    own_weight = pltpu.make_async_copy(w_ref, w_all.at[sp, :, own_lanes], own_sem.at[2])
    for copy in local + [own_weight]:
        copy.start()
    copies = []
    for k, g in others:
        there = lax.rem(zone + k, zones)
        if g == 0:
            copies.append(
                remote(q_ref.at[there], q_all.at[here, :], send_q.at[k], recv_q.at[k], at(k, g))
            )
        copies.append(
            remote(
                kv_ref.at[there], kv_all.at[zone, place],
                send_k.at[k, g], recv_k.at[k, g], at(k, g),
            )
        )

    def weight(k, j, g):
        row = lax.rem(zone - k + zones, zones) * group + lax.rem(place - g + group, group)
        lane = lax.rem(column - j + columns, columns) * cores + core
        return w_all.at[row, :, pl.ds(pl.multiple_of(lane * w_cols, w_cols), w_cols)]

    flights = {}

    def to_core(k, j, g):
        source = w_ref if k + j + g == 0 else weight(k, j, g)
        flights["c", k, j, g] = remote(
            source, weight(k, j, g), send_c.at[k, j, g], recv_c.at[k, j, g], partner
        )

    def to_places(k, j):
        source = w_ref if k + j == 0 else weight(k, j, 0)
        for g in range(1, group):
            flights["y", k, j, g] = remote(
                source, weight(k, j, 0), send_y.at[k, j, g], recv_y.at[k, j, g], at(0, g)
            )
        to_core(k, j, 0)

    def to_columns(k):
        source = w_ref if k == 0 else weight(k, 0, 0)
        for j in range(1, columns):
            flights["x", k, j] = remote(
                source, weight(k, 0, 0), send_x.at[k, j], recv_x.at[k, j], at_column(j)
            )
        to_places(k, 0)

    def zone_event(k):
        flights["z", k].wait_recv()
        to_columns(k)

    def column_event(k):
        for j in range(1, columns):
            flights["x", k, j].wait_recv()
            to_places(k, j)

    def place_event(k):
        for j in range(columns):
            for g in range(1, group):
                flights["y", k, j, g].wait_recv()
                to_core(k, j, g)

    for k in range(1, zones):
        flights["z", k] = remote(w_ref, weight(0, 0, 0), send_z.at[k], recv_z.at[k], at(k, 0))
    to_columns(0)

    for copy in local + copies:
        copy.wait()
    for z in range(zones):
        for g in range(group):
            target = slice((z * group + g) * rows, (z * group + g + 1) * rows)
            first = g * 2 * ck
            parts = [kv_all[z, y] for y in range(group)]
            k_all[target, :] = jnp.concatenate([p[:, first : first + ck] for p in parts], axis=1)
            v_all[target, :] = jnp.concatenate(
                [p[:, first + ck : first + 2 * ck] for p in parts], axis=1
            )

    row = lax.broadcasted_iota(jnp.int32, (block, block), 0)
    lane = lax.broadcasted_iota(jnp.int32, (block, block), 1)
    later = jnp.where(row > lane, 1.0, 0.0).astype(jnp.bfloat16)
    strict = lane < row

    def tile(i, j, h, rest, total, diagonal):
        window = pl.ds(pl.multiple_of(j * block, block), block)
        lanes = slice(h * HEAD_DIM, (h + 1) * HEAD_DIM)
        q = q_all[i * block : (i + 1) * block, lanes] * jnp.bfloat16(HEAD_DIM**-0.5)
        x = lax.dot_general(
            q, k_all[window, :], (((1,), (1,)), ((), ())), preferred_element_type=jnp.float32
        ) + bias_ref[h : h + 1, window]
        soft = jnp.log(1.0 + jnp.exp(-jnp.abs(x)))
        take = jnp.minimum(x, 0.0) - soft
        keep = jnp.minimum(-x, 0.0) - soft
        if diagonal:
            keep = jnp.where(strict, keep, 0.0)
        high = keep.astype(jnp.bfloat16)
        low = (keep - high.astype(jnp.float32)).astype(jnp.bfloat16)
        after = jnp.dot(high, later, preferred_element_type=jnp.float32) + jnp.dot(
            low, later, preferred_element_type=jnp.float32
        )
        sticks = jnp.exp(take + (after + rest))
        if diagonal:
            sticks = jnp.where(strict, sticks, 0.0)
        total = total + jnp.dot(
            sticks.astype(jnp.bfloat16), v_all[window, :], preferred_element_type=jnp.float32
        )
        return rest + (after[:, :1] + keep[:, :1]), total

    events = []
    for n in range(1, zones + 2):
        now = []
        if n < zones:
            now.append(functools.partial(zone_event, n))
        if n <= zones:
            now.append(functools.partial(column_event, n - 1))
        if 0 <= n - 3 < zones:
            now.append(functools.partial(place_event, n - 3))
        events.append((n if n <= 3 else 2 * n - 3, now))
    events.append((10**9, [functools.partial(place_event, zones - 1)]))
    ready = []
    point = [0]

    def send_head(s):
        return pltpu.make_async_remote_copy(
            src_ref=head.at[s * rows : (s + 1) * rows, :], dst_ref=arrived.at[sp],
            send_sem=send_h.at[s], recv_sem=recv_h.at[sp],
            device_id={"sp": s}, device_id_type=MESH,
        )

    def receive_head(s):
        return pltpu.make_async_remote_copy(
            src_ref=head.at[s * rows : (s + 1) * rows, :], dst_ref=arrived.at[s],
            send_sem=send_h.at[s], recv_sem=recv_h.at[s],
            device_id={"sp": s}, device_id_type=MESH,
        )

    def unless_own(s, act):
        @pl.when(sp != s)
        def _():
            act()

    def relay(final=False):
        while events and (final or events[0][0] <= point[0]):
            for event in events.pop(0)[1]:
                event()
        while ready:
            s = ready.pop(0)
            unless_own(s, lambda s=s: send_head(s).start())
        point[0] += 1

    done = 0
    for i in range(length // block):
        state = []
        for h in range(heads):
            state += tile(
                i, i, h, jnp.zeros((block, 1), jnp.float32),
                jnp.zeros((block, HEAD_DIM), jnp.float32), True,
            )
        state = tuple(state)
        begin = 0
        while begin < i:
            end = min(begin + (2 if begin == 0 else 3), i)

            def step(n, state, i=i):
                out = []
                for h in range(heads):
                    out += tile(i, i - 1 - n, h, state[2 * h], state[2 * h + 1], False)
                return tuple(out)

            state = lax.fori_loop(begin, end, step, state)
            begin = end
            if begin < i:
                relay()
        for h in range(heads):
            total = state[2 * h + 1]
            lanes = slice(h * HEAD_DIM, (h + 1) * HEAD_DIM)
            scaled = total * lax.rsqrt(jnp.mean(total * total, axis=-1, keepdims=True) + norm_eps)
            head[i * block : (i + 1) * block, lanes] = (
                scaled * gain_ref[:, lanes]
            ).astype(jnp.bfloat16)
        if i + 1 < length // block:
            relay()
        while (done + 1) * rows <= (i + 1) * block:
            ready.append(done)
            done += 1
    relay(final=True)
    mine = pltpu.make_async_copy(
        head.at[pl.ds(pl.multiple_of(sp * rows, rows), rows), :], arrived.at[sp], own_sem.at[3]
    )
    mine.start()
    own_weight.wait()
    for key, copy in flights.items():
        if key[0] == "c":
            copy.wait_recv()
    mine.wait()
    for s in range(size):
        unless_own(s, lambda s=s: receive_head(s).wait_recv())
    for s in range(size):
        joined[:, s * cq : (s + 1) * cq] = arrived[s]
    wide = min(512, width)

    def multiply(n, carry):
        lanes = pl.ds(pl.multiple_of(n * wide, wide), wide)
        weights = w_all[:, :, lanes].reshape(size * cq, wide)
        out_ref[:, lanes] = jnp.dot(
            joined[...], weights, preferred_element_type=jnp.float32
        ).astype(jnp.bfloat16)
        return carry

    lax.fori_loop(0, width // wide, multiply, 0)
    for copy in flights.values():
        copy.wait_send()
    for s in range(size):
        unless_own(s, lambda s=s: send_head(s).wait_send())


def mixer(q, kv, w_out, bias, gains, zones, group):
    span, cq = q.shape[1:]
    rows = span // group
    size = zones * group
    length = size * rows
    cores = 2
    columns = lax.axis_size("dp") // cores
    width = w_out.shape[1] * columns * cores
    block = min(256, length)
    dma = pltpu.SemaphoreType.DMA
    grid3 = (zones, columns, group)
    return pl.pallas_call(
        functools.partial(mixer_kernel, zones, group, block),
        out_shape=jax.ShapeDtypeStruct((rows, width), jnp.bfloat16),
        in_specs=[VMEM_SPEC] * 5,
        out_specs=VMEM_SPEC,
        scratch_shapes=[
            pltpu.VMEM((length, cq), jnp.bfloat16),
            pltpu.VMEM((zones, group) + kv.shape[1:], jnp.bfloat16),
            pltpu.VMEM((length, HEAD_DIM), jnp.bfloat16),
            pltpu.VMEM((length, HEAD_DIM), jnp.bfloat16),
            pltpu.VMEM((size, w_out.shape[0], width), jnp.bfloat16),
            pltpu.VMEM((length, cq), jnp.bfloat16),
            pltpu.VMEM((size, rows, cq), jnp.bfloat16),
            pltpu.VMEM((rows, size * cq), jnp.bfloat16),
            dma((4,)),
            dma((zones,)), dma((zones,)),
            dma((zones, group)), dma((zones, group)),
            dma((zones,)), dma((zones,)),
            dma((zones, columns)), dma((zones, columns)),
            dma(grid3), dma(grid3), dma(grid3), dma(grid3),
            dma((size,)), dma((size,)),
        ],
        compiler_params=pltpu.CompilerParams(collective_id=1, has_side_effects=True),
        name="mixer",
    )(q, kv, w_out, bias, gains)


def body(inputs, in_gain, w_query, w_key, w_value, key_bias, out_gain, w_out):
    width_sp = lax.axis_size("sp")
    own_index = lax.axis_index("sp")
    cq = w_query.shape[1]
    ck = w_key.shape[1]
    group = HEAD_DIM // ck
    zones = width_sp // group
    depth = w_query.shape[0]
    pair = jnp.concatenate([w_key, w_value], axis=1)
    piece = jnp.concatenate(
        [w_query, jnp.concatenate([pair[: depth // 2], pair[depth // 2 :]], axis=1)], axis=0
    )
    q_parts, kv_parts = project(inputs[0], in_gain[None], piece, zones, group, 2 * ck)
    gains = lax.dynamic_slice_in_dim(out_gain, own_index * cq, cq, 0).reshape(1, cq)
    return mixer(q_parts, kv_parts, w_out, key_bias[0].T, gains, zones, group)[None]


def solution(mesh):
    placed = (
        P("dp", "sp", None),
        P(),
        P("dp", "sp"),
        P("dp", "sp"),
        P("dp", "sp"),
        P("dp", None, "sp"),
        P(),
        P("sp", "dp"),
    )
    return jax.shard_map(
        body, mesh=mesh, in_specs=placed, out_specs=P("dp", "sp", None), check_vma=False
    )
```

profile of v0, /device:TPU:28, one launch (start us, length us, event | category | flops | bytes accessed | tf_op | source)
XLA Modules:
  0.0 108.9 jit_solution(11706991075479092977)
XLA Ops:
  0.0 0.0 copy-start
  0.0 0.7 copy-done
  0.7 0.6 dynamic-slice_bitcast_fusion.gain_ref
  1.3 0.0 copy-start.2
  1.3 0.9 copy.9
  2.2 0.0 copy-done.2
  2.2 0.1 copy.10
  2.3 0.0 copy-start.1
  2.3 0.1 fusion.8
  2.4 0.8 copy-done.1
  3.2 0.8 fusion.7.piece_ref
  4.0 36.7 %project.1 = (bf16[4,384,128]{2,1,0:T(8,128)(2,1)}, bf16[4,192,128]{2,1,0:T(8,128)(2,1)}) custom-call(bf16[192,2048]{1,0:T(8,128)(2,1)} %bitcast.9, f32[1,2048]{1,0:T(1,128)} %bitcast.11, bf16[768,128]{1,0:T(8,128)(2,1)} %fusion.7.piece_ref), custom_call_target="tpu_custom_call" | custom-call | tf_op jit(solution)/shard_map/project/pallas_call | solution.py:189
  40.8 66.1 %mixer.1 = bf16[192,2048]{1,0:T(8,128)(2,1)} custom-call(bf16[4,384,128]{2,1,0:T(8,128)(2,1)} %get-tuple-element.7.q_ref, bf16[4,192,128]{2,1,0:T(8,128)(2,1)} %get-tuple-element.8.kv_ref, bf16[128,512]{1,0:T(8,128)(2,1)} %w_ref.1, f32[2,1536]{1,0:T(2,128)} %bitcast.10, f32[1,128]{1,0:T(1,128)} %dynamic-slice_bitcast_fusion.gain_ref), custom_call_target="tpu_custom_call" | custom-call | tf_op jit(solution)/shard_map/mixer/pallas_call | solution.py:474
  106.8 2.1 %copy.12 = bf16[1,192,2048]{2,1,0:T(8,128)(2,1)} copy(bf16[1,192,2048]{2,1,0:T(8,128)(2,1)} %bitcast.8) | data formatting | bytes 1572864
Async XLA Ops:
  0.0 0.7 copy-start
  1.3 0.9 copy-start.2
  2.3 0.9 copy-start.1
where the time goes:
time: 109 us
  Pallas kernels  103 us (94%)
  local copies, waits for them, and re-layouts  5.19 us (5%)
    pallas_call x1, Pallas kernels, mixer(): pl.pallas_call(functools.partial(mixer_kernel, zones, group, block), out_...  66.1 us
    pallas_call x1, Pallas kernels, project(): pl.pallas_call(functools.partial(project_kernel, zones, group), out_shape...  36.7 us
    unnamed x9, local copies, waits for them, and re-layouts  4.59 us

commit v1 on v0

v1 whole, which is shorter than its diff:
```python
import functools
import math

import jax
import jax.numpy as jnp
from jax import lax
from jax.experimental import pallas as pl
from jax.experimental.pallas import tpu as pltpu
from jax.sharding import PartitionSpec as P

HEAD_DIM = 64
LOG2E = math.log2(math.e)
MESH = pl.DeviceIdType.MESH
VMEM_SPEC = pl.BlockSpec(memory_space=pltpu.VMEM)
f32, bf16 = jnp.float32, jnp.bfloat16


norm_eps = 1e-06
cores = 2
chunks = 2
aug = 16


def remote(source, target, send, recv, peer):
    copy = pltpu.make_async_remote_copy(
        src_ref=source, dst_ref=target, send_sem=send, recv_sem=recv,
        device_id=peer, device_id_type=MESH,
    )
    return copy


def layer_kernel(
    zones, group,
    x_ref, in_gain_ref, wq_ref, wk_ref, wv_ref, bias_ref, out_gain_ref, w_ref, out_ref,
    weights, x_far, normed, outbox, inbox, kvbox, k_aug, v_t, q_t, rest, total, tri,
    w_all, head, arrived, joined,
    own_sem, send_z, recv_z, send_x, recv_x, send_c, recv_c, send_y, recv_y,
    send_m, recv_m, send_k, recv_k,
    send_wz, recv_wz, send_wa, recv_wa, send_wb, recv_wb, send_wc, recv_wc, send_h, recv_h,
):
    columns = lax.axis_size("dp") // cores
    sp, dp = lax.axis_index("sp"), lax.axis_index("dp")
    zone, place = sp // group, sp % group
    column, core = dp // cores, dp % cores
    rows, width = x_ref.shape
    size = zones * group
    span = group * rows
    pieces = columns * cores
    depth = width // pieces
    half = depth // 2
    cq = wq_ref.shape[1]
    ck = wk_ref.shape[0]
    ck2 = 2 * ck
    fold = cq // ck2
    heads = bias_ref.shape[0]
    wide = heads * span
    length = size * rows
    piece_rows = weights.shape[2]
    part = piece_rows // chunks
    w_cols = w_ref.shape[1]
    log_zones = range(1, zones)

    below, above = zone, zones - 1 - zone
    near = jnp.minimum(below, above)
    toward = jnp.where(below <= above, -1, 1)

    def source(n):
        if n == 0:
            return zone
        sign = toward if n % 2 == 1 else -toward
        offset = jnp.where(n <= 2 * near, sign * ((n + 1) // 2), -toward * (n - near))
        return zone + offset

    def at_zone(z):
        return {"sp": z * group + place}

    def at_column(j):
        return {"dp": lax.rem(column + j, columns) * cores + core}

    def at_place(g):
        return {"sp": zone * group + lax.rem(place + g, group)}

    def token_place(g):
        return lax.rem(place - g + group, group)

    partner = {"dp": column * cores + (1 - core)}

    barrier = pltpu.get_barrier_semaphore()
    peers = [
        {"sp": lax.rem(sp + k, size)} for k in range(1, size)
    ] + [at_column(j) for j in range(1, columns)] + [partner]
    for peer in peers:
        pl.semaphore_signal(barrier, inc=1, device_id=peer, device_id_type=MESH)

    pair = jnp.concatenate([wk_ref[...].astype(f32), wv_ref[...].astype(f32)], axis=0).T
    weights[zone, 0, :depth, :] = wq_ref[...]
    weights[zone, 0, depth:, :] = jnp.concatenate([pair[:half], pair[half:]], axis=1).astype(bf16)

    below_diag = lax.broadcasted_iota(jnp.int32, (rows, rows), 1) >= lax.broadcasted_iota(
        jnp.int32, (rows, rows), 0
    )
    tri[...] = jnp.where(below_diag, -1.0, 0.0).astype(bf16)
    mark_row = lax.broadcasted_iota(jnp.int32, (aug, wide), 0)
    mark_head = lax.broadcasted_iota(jnp.int32, (aug, wide), 1) // span
    marks = jnp.where(
        (mark_row >= 3 * mark_head) & (mark_row < 3 * mark_head + 3), 1.0, 0.0
    ).astype(bf16)
    for z in range(zones):
        q_t[z, 2 * HEAD_DIM :, :] = marks
    row_of = lax.broadcasted_iota(jnp.int32, (8, span), 0)
    for z in range(zones):
        tokens = slice(z * span, (z + 1) * span)
        terms = jnp.zeros((8, span), f32)
        for h in range(heads):
            value = bias_ref[h : h + 1, tokens] * LOG2E
            high = value.astype(bf16).astype(f32)
            middle = (value - high).astype(bf16).astype(f32)
            low = value - high - middle
            for i, term in enumerate((high, middle, low)):
                terms = jnp.where(row_of == 3 * h + i, term, terms)
        padded = jnp.concatenate([terms, jnp.zeros((120, span), f32)], axis=0)
        k_aug[tokens, 128:256] = padded.T.astype(bf16)

    pl.semaphore_wait(barrier, len(peers))

    z_copies, x_copies, c_copies = [], {}, {}

    def piece(z, d, c):
        return weights.at[z, d, pl.ds(c * part, part), :]

    def send_outward(n, z, sender):
        for way, target in ((0, zone - 1), (1, zone + 1)):
            exists = (target >= 0) if way == 0 else (target < zones)
            if n > 0:
                exists = exists & ((z > zone) if way == 0 else (z < zone))
            yield way, target, exists

    def z_send(n, c, way, target):
        z = source(n)
        return remote(
            piece(z, 0, c), piece(z, 0, c), send_z.at[n, c, way], recv_z.at[z, c], at_zone(target)
        )

    def z_relay(n, c, act):
        for way, target, exists in send_outward(n, source(n), None):
            copy = z_send(n, c, way, jnp.clip(target, 0, zones - 1))

            @pl.when(exists)
            def _(copy=copy):
                act(copy)

    def z_wait(n, c):
        z = source(n)
        remote(
            piece(z, 0, c), piece(z, 0, c), send_z.at[n, c, 0], recv_z.at[z, c], at_zone(zone)
        ).wait_recv()

    def spread(n, c):
        z = source(n)
        for j in range(1, columns):
            x_copies[n, j, c] = remote(
                piece(z, 0, c), piece(z, cores * j, c),
                send_x.at[n, j, c], recv_x.at[n, j, c], at_column(j),
            )
            x_copies[n, j, c].start()
        c_copies[n, 0, c] = remote(
            piece(z, 0, c), piece(z, 1, c), send_c.at[n, 0, c], recv_c.at[n, 0, c], partner
        )
        c_copies[n, 0, c].start()

    def spread_columns(n):
        z = source(n)
        for c in range(chunks):
            for j in range(1, columns):
                x_copies[n, j, c].wait_recv()
                c_copies[n, j, c] = remote(
                    piece(z, cores * j, c), piece(z, cores * j + 1, c),
                    send_c.at[n, j, c], recv_c.at[n, j, c], partner,
                )
                c_copies[n, j, c].start()

    def arrive(n):
        for c in range(chunks):
            if n > 0:
                z_wait(n, c)
            z_relay(n, c, lambda copy: copy.start())
            spread(n, c)

    def normalize(rows_ref, g):
        step = 16

        def chunk(i, carry):
            here = pl.ds(pl.multiple_of(i * step, step), step)
            full = rows_ref[here, :].astype(f32)
            scale = lax.rsqrt(jnp.mean(full * full, axis=-1, keepdims=True) + norm_eps)
            for d in range(pieces):
                j, c = d // cores, d % cores
                index = lax.rem(column - j + columns, columns) * cores + (
                    core if c == 0 else 1 - core
                )
                for s in range(2):
                    lanes = pl.ds(pl.multiple_of(index * depth + s * half, half), half)
                    some = rows_ref[here, lanes].astype(f32) * scale * in_gain_ref[:, lanes]
                    normed[g, s, here, d * half : (d + 1) * half] = some.astype(bf16)
            return carry

        lax.fori_loop(0, rows // step, chunk, 0)

    m_copies, k_copies = [], {}

    def project(n, g):
        z = source(n)
        key_weights = weights[z, :, depth : depth + half, :].reshape(pieces * half, cq)
        both = []
        for s in range(2):
            query_weights = weights[z, :, s * half : (s + 1) * half, :].reshape(pieces * half, cq)
            both.append(
                jnp.dot(
                    normed[g, s], jnp.concatenate([query_weights, key_weights], axis=1),
                    preferred_element_type=f32,
                )
            )
        q = (both[0][:, :cq] + both[1][:, :cq]).astype(bf16)
        kv = both[0][:, cq : cq + ck2] + both[1][:, cq + ck2 : cq + 2 * ck2]
        deep = rows // fold
        kv = jnp.concatenate(
            [kv[i * deep : (i + 1) * deep] for i in range(fold)], axis=1
        ).astype(bf16)
        tokens = token_place(g)
        if n == 0:
            inbox[zone, tokens, :rows, :] = q
            inbox[zone, tokens, rows:, :] = kv
        else:
            outbox[n, g, :rows, :] = q
            outbox[n, g, rows:, :] = kv
            copy = remote(
                outbox.at[n, g], inbox.at[zone, tokens],
                send_m.at[n, g], recv_m.at[zone, tokens], at_zone(z),
            )
            copy.start()
            m_copies.append(copy)

    def share_keys(n, g):
        z, tokens = source(n), token_place(g)
        if n > 0:
            remote(
                inbox.at[z, tokens], inbox.at[z, tokens],
                send_m.at[n, g], recv_m.at[z, tokens], at_zone(zone),
            ).wait_recv()
        for i in range(1, group):
            copy = remote(
                inbox.at[z, tokens, pl.ds(rows, rows // fold), :], kvbox.at[z, tokens, place],
                send_k.at[n, g, i], recv_k.at[z, tokens, place], at_place(i),
            )
            copy.start()
            k_copies[n, g, i] = copy
        kvbox[z, tokens, place] = inbox[z, tokens, rows:, :]

    def collect(n):
        z = source(n)
        for t in range(group):
            for i in range(1, group):
                owner = token_place(i)
                remote(
                    kvbox.at[z, t, owner], kvbox.at[z, t, owner],
                    send_k.at[n, 0, i], recv_k.at[z, t, owner], at_place(i),
                ).wait_recv()
        for t in range(group):
            parts = []
            for p in range(group):
                packed = kvbox[z, t, p].astype(f32)
                parts.append(
                    jnp.concatenate(
                        [packed[:, i * ck2 : (i + 1) * ck2] for i in range(fold)], axis=0
                    )
                )
            keys = [p[:, :ck] for p in parts]
            values = [p[:, ck:] for p in parts]
            target = pl.ds(pl.multiple_of((z * group + t) * rows, rows), rows)
            k_aug[target, 0:128] = jnp.concatenate(keys + keys, axis=1).astype(bf16)
            turned = jnp.concatenate(keys + values, axis=1).T
            v_t[z * group + t] = turned[HEAD_DIM:].astype(bf16)
        q = jnp.concatenate(
            [inbox[z, t, :rows, :].astype(f32) for t in range(group)], axis=0
        )
        turned = q.T * (LOG2E * HEAD_DIM**-0.5)
        high = turned.astype(bf16)
        low = (turned - high.astype(f32)).astype(bf16)
        for h in range(heads):
            lanes = slice(h * span, (h + 1) * span)
            own = slice(h * HEAD_DIM, (h + 1) * HEAD_DIM)
            q_t[z, :HEAD_DIM, lanes] = high[own]
            q_t[z, HEAD_DIM : 2 * HEAD_DIM, lanes] = low[own]

    def attend(qz, kz, diagonal):
        after = None if diagonal else rest[qz]
        acc = None if diagonal else total[qz]
        logits = {}
        for t in reversed(range(group)):
            window = pl.ds(pl.multiple_of((kz * group + t) * rows, rows), rows)
            logits[t] = jnp.dot(
                k_aug[window, : 2 * HEAD_DIM + aug], q_t[qz], preferred_element_type=f32
            )
        for t in reversed(range(group)):
            x = logits[t]
            soft = jnp.maximum(x, lax.log2(1.0 + lax.exp2(jnp.minimum(x, 126.0))))
            if diagonal:
                key = lax.broadcasted_iota(jnp.int32, (rows, wide), 0) + t * rows
                query = lax.rem(lax.broadcasted_iota(jnp.int32, (rows, wide), 1), span)
                strict = key < query
                soft = jnp.where(strict, soft, 0.0)
            kept = jnp.dot(tri[...], soft.astype(bf16), preferred_element_type=f32)
            power = x + kept
            if after is not None:
                power = power + after
            sticks = lax.exp2(power)
            if diagonal:
                sticks = jnp.where(strict, sticks, 0.0)
            more = jnp.dot(v_t[kz * group + t], sticks.astype(bf16), preferred_element_type=f32)
            acc = more if acc is None else acc + more
            after = kept[0:1, :] if after is None else after + kept[0:1, :]
        total[qz] = acc
        rest[qz] = after

    def send_head(s):
        return remote(
            head.at[pl.ds(s * rows, rows), :], arrived.at[sp],
            send_h.at[s], recv_h.at[sp], {"sp": s},
        )

    def receive_head(s):
        return remote(
            head.at[pl.ds(s * rows, rows), :], arrived.at[s],
            send_h.at[s], recv_h.at[s], {"sp": s},
        )

    def finish(qz):
        scaled = []
        for h in range(heads):
            some = total[qz, :, h * span : (h + 1) * span]
            scaled.append(
                some * lax.rsqrt(jnp.mean(some * some, axis=0, keepdims=True) + norm_eps)
            )
        lanes = pl.ds(pl.multiple_of(sp * cq, cq), cq) if cq % 128 == 0 else None
        gains = own_gain() if lanes is None else out_gain_ref[:, lanes]
        here = pl.ds(pl.multiple_of(qz * span, span), span)
        head[here, :] = (jnp.concatenate(scaled, axis=0).T * gains).astype(bf16)
        for t in range(group):
            s = qz * group + t

            @pl.when(s != sp)
            def _(s=s):
                send_head(s).start()

    def own_gain():
        both = out_gain_ref[:, pl.ds(pl.multiple_of(sp // 2 * 128, 128), 128)]
        return jnp.where(sp % 2 == 0, both[:, :cq], both[:, cq : 2 * cq])

    balanced = columns == group
    lean = core if balanced else 0

    def weight(n, j, i):
        dx = j * (1 - lean) + i * lean
        dy = j * lean + i * (1 - lean)
        row = source(n) * group + lax.rem(place - dy + group, group)
        lane = lax.rem(column - dx + columns, columns) * cores + core
        return w_all.at[row, :, pl.ds(pl.multiple_of(lane * w_cols, w_cols), w_cols)]

    first_count = columns if not balanced else group
    second_count = group if not balanced else columns

    def at_first(j):
        return {
            "sp": zone * group + lax.rem(place + j * lean, group),
            "dp": lax.rem(column + j * (1 - lean), columns) * cores + core,
        }

    def at_second(i):
        return {
            "sp": zone * group + lax.rem(place + i * (1 - lean), group),
            "dp": lax.rem(column + i * lean, columns) * cores + core,
        }

    flights = {}

    def w_core(n, j, i):
        flights["c", n, j, i] = remote(
            weight(n, j, i), weight(n, j, i), send_wc.at[n, j, i], recv_wc.at[n, j, i], partner
        )
        flights["c", n, j, i].start()

    def w_second(n, j):
        for i in range(1, second_count):
            flights["b", n, j, i] = remote(
                weight(n, j, 0), weight(n, j, 0),
                send_wb.at[n, j, i], recv_wb.at[n, j, i], at_second(i),
            )
            flights["b", n, j, i].start()
        w_core(n, j, 0)

    def w_first(n):
        for j in range(1, first_count):
            flights["a", n, j] = remote(
                weight(n, 0, 0), weight(n, 0, 0),
                send_wa.at[n, j], recv_wa.at[n, j], at_first(j),
            )
            flights["a", n, j].start()
        w_second(n, 0)

    def wz_relay(n, act):
        z = source(n)
        for way, target, exists in send_outward(n, z, None):
            copy = remote(
                weight(n, 0, 0), weight(n, 0, 0), send_wz.at[n, way], recv_wz.at[z],
                at_zone(jnp.clip(target, 0, zones - 1)),
            )

            @pl.when(exists)
            def _(copy=copy):
                act(copy)

    def w_zone_event(n):
        z = source(n)
        remote(
            weight(n, 0, 0), weight(n, 0, 0), send_wz.at[n, 0], recv_wz.at[z], at_zone(zone)
        ).wait_recv()
        wz_relay(n, lambda copy: copy.start())
        w_first(n)

    def w_first_event(n):
        for j in range(1, first_count):
            flights["a", n, j].wait_recv()
            w_second(n, j)

    def w_second_event(n):
        for j in range(first_count):
            for i in range(1, second_count):
                flights["b", n, j, i].wait_recv()
                w_core(n, j, i)

    arrive(0)
    place_copies = []
    for g in range(1, group):
        copy = remote(x_ref, x_far.at[g - 1], send_y.at[g], recv_y.at[g], at_place(g))
        copy.start()
        place_copies.append(copy)
    own_weight = pltpu.make_async_copy(w_ref, weight(0, 0, 0), own_sem)
    own_weight.start()
    normalize(x_ref, 0)

    def settle(n):
        for j in range(columns):
            for c in range(chunks):
                c_copies[n, j, c].wait_recv()

    for n in range(1, zones):
        arrive(n)
        spread_columns(n - 1)
        if n > 1:
            settle(n - 2)
            project(n - 2, 0)
    own_weight.wait()
    wz_relay(0, lambda copy: copy.start())
    settle(zones - 2)
    project(zones - 2, 0)
    for g in range(1, group):
        place_copies[g - 1].wait_recv()
        normalize(x_far.at[g - 1], g)
        for n in range(zones - 1):
            project(n, g)
    for g in range(group):
        share_keys(0, g)
    spread_columns(zones - 1)
    settle(zones - 1)
    for g in range(group):
        project(zones - 1, g)
    w_first(0)

    events = []
    for n in range(1, zones):
        events.append([functools.partial(w_zone_event, n), functools.partial(w_first_event, n - 1)])
    events.append([functools.partial(w_first_event, zones - 1)])

    for n in range(zones):
        if n + 1 < zones:
            for g in range(group):
                share_keys(n + 1, g)
        collect(n)
        a = source(n)
        upward = a > zone if n > 0 else None
        attend(a, a, True)
        if n == 0:
            tiles = [(a, a)]
        else:
            tiles = [(a, a)] + [
                (jnp.where(upward, a, a + m), jnp.where(upward, a - m, a)) for m in range(1, n + 1)
            ]
        for m, (qz, kz) in enumerate(tiles):
            if m > 0:
                attend(qz, kz, False)

            @pl.when(kz == 0)
            def _(qz=qz):
                finish(qz)
        if events:
            for event in events.pop(0):
                event()
    while events:
        for event in events.pop(0):
            event()
    for n in range(zones):
        w_second_event(n)
    mine = pltpu.make_async_copy(
        head.at[pl.ds(pl.multiple_of(sp * rows, rows), rows), :], arrived.at[sp], own_sem
    )
    mine.start()
    for key, copy in flights.items():
        if key[0] == "c":
            copy.wait_recv()
    mine.wait()
    for s in range(size):
        @pl.when(sp != s)
        def _(s=s):
            receive_head(s).wait_recv()
    for s in range(size):
        joined[:, s * cq : (s + 1) * cq] = arrived[s]
    strip = min(512, width)

    def multiply(i, carry):
        lanes = pl.ds(pl.multiple_of(i * strip, strip), strip)
        out_ref[:, lanes] = jnp.dot(
            joined[...], w_all[:, :, lanes].reshape(size * cq, strip), preferred_element_type=f32
        ).astype(bf16)
        return carry

    lax.fori_loop(0, width // strip, multiply, 0)
    for n in range(zones):
        for c in range(chunks):
            z_relay(n, c, lambda copy: copy.wait_send())
        wz_relay(n, lambda copy: copy.wait_send())
    for copies in (x_copies, c_copies, k_copies, flights):
        for copy in copies.values():
            copy.wait_send()
    for copy in place_copies + m_copies:
        copy.wait_send()
    for s in range(size):
        @pl.when(sp != s)
        def _(s=s):
            send_head(s).wait_send()


def layer(x, in_gain, wq, wk, wv, bias, out_gain, w_out, zones, group):
    rows, width = x.shape
    pieces = lax.axis_size("dp")
    columns = pieces // cores
    size = zones * group
    span = group * rows
    length = size * rows
    depth, cq = wq.shape
    ck2 = 2 * wk.shape[0]
    fold = cq // ck2
    heads = bias.shape[0]
    wide = heads * span
    message = rows + rows // fold
    dma = pltpu.SemaphoreType.DMA
    most = max(columns, group)
    return pl.pallas_call(
        functools.partial(layer_kernel, zones, group),
        out_shape=jax.ShapeDtypeStruct((rows, width), bf16),
        in_specs=[VMEM_SPEC] * 8,
        out_specs=VMEM_SPEC,
        scratch_shapes=[
            pltpu.VMEM((zones, pieces, depth + depth // 2, cq), bf16),
            pltpu.VMEM((group - 1, rows, width), bf16),
            pltpu.VMEM((group, 2, rows, width // 2), bf16),
            pltpu.VMEM((zones, group, message, cq), bf16),
            pltpu.VMEM((zones, group, message, cq), bf16),
            pltpu.VMEM((zones, group, group, rows // fold, cq), bf16),
            pltpu.VMEM((length, 256), bf16),
            pltpu.VMEM((size, HEAD_DIM, rows), bf16),
            pltpu.VMEM((zones, 2 * HEAD_DIM + aug, wide), bf16),
            pltpu.VMEM((zones, 1, wide), f32),
            pltpu.VMEM((zones, HEAD_DIM, wide), f32),
            pltpu.VMEM((rows, rows), bf16),
            pltpu.VMEM((size, w_out.shape[0], width), bf16),
            pltpu.VMEM((length, cq), bf16),
            pltpu.VMEM((size, rows, cq), bf16),
            pltpu.VMEM((rows, size * cq), bf16),
            dma,
            dma((zones, chunks, 2)), dma((zones, chunks)),
            dma((zones, columns, chunks)), dma((zones, columns, chunks)),
            dma((zones, columns, chunks)), dma((zones, columns, chunks)),
            dma((group,)), dma((group,)),
            dma((zones, group)), dma((zones, group)),
            dma((zones, group, group)), dma((zones, group, group)),
            dma((zones, 2)), dma((zones,)),
            dma((zones, most)), dma((zones, most)),
            dma((zones, most, most)), dma((zones, most, most)),
            dma((zones, most, most)), dma((zones, most, most)),
            dma((size,)), dma((size,)),
        ],
        compiler_params=pltpu.CompilerParams(collective_id=0, has_side_effects=True),
        name="layer",
    )(x, in_gain, wq, wk, wv, bias, out_gain, w_out)


def body(inputs, in_gain, w_query, w_key, w_value, key_bias, out_gain, w_out):
    group = HEAD_DIM // w_key.shape[1]
    zones = lax.axis_size("sp") // group
    return layer(
        inputs[0], in_gain[None], w_query, w_key.T, w_value.T, key_bias[0].T,
        out_gain[None], w_out, zones, group,
    )[None]


def solution(mesh):
    placed = (
        P("dp", "sp", None),
        P(),
        P("dp", "sp"),
        P("dp", "sp"),
        P("dp", "sp"),
        P("dp", None, "sp"),
        P(),
        P("sp", "dp"),
    )
    return jax.shard_map(
        body, mesh=mesh, in_specs=placed, out_specs=P("dp", "sp", None), check_vma=False
    )
```

time: 109 us -> 70.1 us (0.64)
  the two profiles are of different devices: /device:TPU:28 before, /device:TPU:1 now
where the time goes in v1:
time: 70.1 us; the launch traced here: 69.9 us
  Pallas kernels  67.8 us (97%)
  local copies, waits for them, and re-layouts  2.09 us (3%)
    pallas_call x1, Pallas kernels, layer(): pl.pallas_call(functools.partial(layer_kernel, zones, group), out_shape=j...  67.8 us
    unnamed x1, local copies, waits for them, and re-layouts  2.09 us

profile of v1, /device:TPU:1, one launch (start us, length us, event | category | flops | bytes accessed | tf_op | source)
XLA Modules:
  0.0 69.9 jit_solution(3638930812175639595)
XLA Ops:
  0.0 67.8 %layer.1 = bf16[192,2048]{1,0:T(8,128)(2,1)} custom-call(bf16[192,2048]{1,0:T(8,128)(2,1)} %bitcast.10, f32[1,2048]{1,0:T(1,128)} %bitcast.14, bf16[512,128]{1,0:T(8,128)(2,1)} %wq_ref.1, bf16[32,512]{1,0:T(8,128)(2,1)} %bitcast.11, bf16[32,512]{1,0:T(8,128)(2,1)} %bitcast.12, f32[2,1536]{1,0:T(2,128)} %bitcast.13, f32[1,1024]{1,0:T(1,128)} %bitcast.15, ...), custom_call_target="tpu_custom_call" | custom-call | tf_op jit(solution)/shard_map/layer/pallas_call | solution.py:567
  67.8 2.1 %copy.10 = bf16[1,192,2048]{2,1,0:T(8,128)(2,1)} copy(bf16[1,192,2048]{2,1,0:T(8,128)(2,1)} %bitcast.9) | data formatting | bytes 1572864

commit v2 on v1

--- a/solution.py
+++ b/solution.py
@@ -31,10 +31,10 @@
 
 def layer_kernel(
     zones, group,
-    x_ref, in_gain_ref, wq_ref, wk_ref, wv_ref, bias_ref, out_gain_ref, w_ref, out_ref,
-    weights, x_far, normed, outbox, inbox, kvbox, k_aug, v_t, q_t, rest, total, tri,
+    x_hbm, in_gain_ref, wq_ref, wk_ref, wv_ref, bias_ref, out_gain_ref, w_ref, out_hbm,
+    x_ref, out_ref, weights, x_far, normed, outbox, inbox, kvbox, k_aug, v_t, q_t, rest, total, tri,
     w_all, head, arrived, joined,
-    own_sem, send_z, recv_z, send_x, recv_x, send_c, recv_c, send_y, recv_y,
+    own_sem, x_sem, out_sem, send_z, recv_z, send_x, recv_x, send_c, recv_c, send_y, recv_y,
     send_m, recv_m, send_k, recv_k,
     send_wz, recv_wz, send_wa, recv_wa, send_wb, recv_wb, send_wc, recv_wc, send_h, recv_h,
 ):
@@ -58,7 +58,6 @@
     piece_rows = weights.shape[2]
     part = piece_rows // chunks
     w_cols = w_ref.shape[1]
-    log_zones = range(1, zones)
 
     below, above = zone, zones - 1 - zone
     near = jnp.minimum(below, above)
@@ -91,6 +90,9 @@
     ] + [at_column(j) for j in range(1, columns)] + [partner]
     for peer in peers:
         pl.semaphore_signal(barrier, inc=1, device_id=peer, device_id_type=MESH)
+
+    x_copy = pltpu.make_async_copy(x_hbm, x_ref, x_sem)
+    x_copy.start()
 
     pair = jnp.concatenate([wk_ref[...].astype(f32), wv_ref[...].astype(f32)], axis=0).T
     weights[zone, 0, :depth, :] = wq_ref[...]
@@ -419,13 +421,33 @@
             def _(copy=copy):
                 act(copy)
 
-    def w_zone_event(n):
-        z = source(n)
-        remote(
-            weight(n, 0, 0), weight(n, 0, 0), send_wz.at[n, 0], recv_wz.at[z], at_zone(zone)
-        ).wait_recv()
-        wz_relay(n, lambda copy: copy.start())
-        w_first(n)
+    middle_zone = near > 0
+
+    def wz_own(n):
+        short = jnp.maximum(2 * near - 1, 0)
+        for way, target, last in (
+            (0, zone - 1, jnp.where(above < below, short, zones - 1)),
+            (1, zone + 1, jnp.where(below <= above, short, zones - 1)),
+        ):
+            exists = (target >= 0) if way == 0 else (target < zones)
+            copy = remote(
+                weight(0, 0, 0), weight(0, 0, 0), send_wz.at[0, way], recv_wz.at[zone],
+                at_zone(jnp.clip(target, 0, zones - 1)),
+            )
+
+            @pl.when(exists & (last == n))
+            def _(copy=copy):
+                copy.start()
+
+    def wz_pass(n, now):
+        z = source(n)
+
+        @pl.when(now)
+        def _():
+            remote(
+                weight(n, 0, 0), weight(n, 0, 0), send_wz.at[n, 0], recv_wz.at[z], at_zone(zone)
+            ).wait_recv()
+            wz_relay(n, lambda copy: copy.start())
 
     def w_first_event(n):
         for j in range(1, first_count):
@@ -438,31 +460,43 @@
                 flights["b", n, j, i].wait_recv()
                 w_core(n, j, i)
 
+    def settle(n):
+        for j in range(columns):
+            for c in range(chunks):
+                c_copies[n, j, c].wait_recv()
+
+    def ready(n):
+        spread_columns(n)
+        settle(n)
+
+    own_weight = pltpu.make_async_copy(w_ref, weight(0, 0, 0), own_sem)
+    own_weight.start()
     arrive(0)
+    own_weight.wait()
+    wz_own(0)
+    x_copy.wait()
     place_copies = []
     for g in range(1, group):
         copy = remote(x_ref, x_far.at[g - 1], send_y.at[g], recv_y.at[g], at_place(g))
         copy.start()
         place_copies.append(copy)
-    own_weight = pltpu.make_async_copy(w_ref, weight(0, 0, 0), own_sem)
-    own_weight.start()
     normalize(x_ref, 0)
-
-    def settle(n):
-        for j in range(columns):
-            for c in range(chunks):
-                c_copies[n, j, c].wait_recv()
-
-    for n in range(1, zones):
+    for n in range(1, zones - 1):
         arrive(n)
-        spread_columns(n - 1)
-        if n > 1:
-            settle(n - 2)
-            project(n - 2, 0)
-    own_weight.wait()
-    wz_relay(0, lambda copy: copy.start())
-    settle(zones - 2)
-    project(zones - 2, 0)
+        wz_own(n)
+    ready(0)
+    project(0, 0)
+    arrive(zones - 1)
+    wz_own(zones - 1)
+    w_first(0)
+    wz_pass(1, middle_zone)
+    for n in range(1, zones - 1):
+        ready(n)
+        project(n, 0)
+    wz_pass(1, jnp.logical_not(middle_zone))
+    w_first(1)
+    for n in range(2, zones - 1):
+        wz_pass(n, middle_zone)
     for g in range(1, group):
         place_copies[g - 1].wait_recv()
         normalize(x_far.at[g - 1], g)
@@ -470,16 +504,25 @@
             project(n, g)
     for g in range(group):
         share_keys(0, g)
-    spread_columns(zones - 1)
-    settle(zones - 1)
+    wz_pass(zones - 1, middle_zone)
+    ready(zones - 1)
     for g in range(group):
         project(zones - 1, g)
-    w_first(0)
-
-    events = []
-    for n in range(1, zones):
-        events.append([functools.partial(w_zone_event, n), functools.partial(w_first_event, n - 1)])
-    events.append([functools.partial(w_first_event, zones - 1)])
+    w_first_event(0)
+
+    def late(n):
+        wz_pass(n, jnp.logical_not(middle_zone))
+        w_first(n)
+
+    for n in range(2, zones - 1):
+        late(n)
+    events = [
+        [(w_first_event, 1), (late, zones - 1)],
+        [(w_first_event, 2), (w_second_event, 0), (w_second_event, 1)],
+    ]
+    for n in range(3, zones):
+        events.append([(w_first_event, n), (w_second_event, n - 1)])
+    events.append([(w_second_event, zones - 1)])
 
     for n in range(zones):
         if n + 1 < zones:
@@ -503,20 +546,28 @@
             def _(qz=qz):
                 finish(qz)
         if events:
-            for event in events.pop(0):
-                event()
+            for event, k in events.pop(0):
+                event(k)
     while events:
-        for event in events.pop(0):
-            event()
-    for n in range(zones):
-        w_second_event(n)
+        for event, k in events.pop(0):
+            event(k)
     mine = pltpu.make_async_copy(
         head.at[pl.ds(pl.multiple_of(sp * rows, rows), rows), :], arrived.at[sp], own_sem
     )
     mine.start()
+    for n in range(zones):
+        for c in range(chunks):
+            z_relay(n, c, lambda copy: copy.wait_send())
+    for copies in (x_copies, c_copies, k_copies):
+        for copy in copies.values():
+            copy.wait_send()
+    for copy in place_copies + m_copies:
+        copy.wait_send()
+    for n in range(zones):
+        wz_relay(n, lambda copy: copy.wait_send())
     for key, copy in flights.items():
-        if key[0] == "c":
-            copy.wait_recv()
+        if key[0] != "c":
+            copy.wait_send()
     mine.wait()
     for s in range(size):
         @pl.when(sp != s)
@@ -524,29 +575,30 @@
             receive_head(s).wait_recv()
     for s in range(size):
         joined[:, s * cq : (s + 1) * cq] = arrived[s]
+    for key, copy in flights.items():
+        if key[0] == "c":
+            copy.wait_recv()
     strip = min(512, width)
 
-    def multiply(i, carry):
-        lanes = pl.ds(pl.multiple_of(i * strip, strip), strip)
+    def put(i):
+        lanes = pl.ds(i * strip, strip)
+        return pltpu.make_async_copy(out_ref.at[:, lanes], out_hbm.at[:, lanes], out_sem.at[i])
+
+    for i in range(width // strip):
+        lanes = slice(i * strip, (i + 1) * strip)
         out_ref[:, lanes] = jnp.dot(
             joined[...], w_all[:, :, lanes].reshape(size * cq, strip), preferred_element_type=f32
         ).astype(bf16)
-        return carry
-
-    lax.fori_loop(0, width // strip, multiply, 0)
-    for n in range(zones):
-        for c in range(chunks):
-            z_relay(n, c, lambda copy: copy.wait_send())
-        wz_relay(n, lambda copy: copy.wait_send())
-    for copies in (x_copies, c_copies, k_copies, flights):
-        for copy in copies.values():
+        put(i).start()
+    for key, copy in flights.items():
+        if key[0] == "c":
             copy.wait_send()
-    for copy in place_copies + m_copies:
-        copy.wait_send()
     for s in range(size):
         @pl.when(sp != s)
         def _(s=s):
             send_head(s).wait_send()
+    for i in range(width // strip):
+        put(i).wait()
 
 
 def layer(x, in_gain, wq, wk, wv, bias, out_gain, w_out, zones, group):
@@ -567,9 +619,11 @@
     return pl.pallas_call(
         functools.partial(layer_kernel, zones, group),
         out_shape=jax.ShapeDtypeStruct((rows, width), bf16),
-        in_specs=[VMEM_SPEC] * 8,
-        out_specs=VMEM_SPEC,
+        in_specs=[pl.BlockSpec(memory_space=pl.ANY)] + [VMEM_SPEC] * 7,
+        out_specs=pl.BlockSpec(memory_space=pl.ANY),
         scratch_shapes=[
+            pltpu.VMEM((rows, width), bf16),
+            pltpu.VMEM((rows, width), bf16),
             pltpu.VMEM((zones, pieces, depth + depth // 2, cq), bf16),
             pltpu.VMEM((group - 1, rows, width), bf16),
             pltpu.VMEM((group, 2, rows, width // 2), bf16),
@@ -586,7 +640,7 @@
             pltpu.VMEM((length, cq), bf16),
             pltpu.VMEM((size, rows, cq), bf16),
             pltpu.VMEM((rows, size * cq), bf16),
-            dma,
+            dma, dma, dma((width // min(512, width),)),
             dma((zones, chunks, 2)), dma((zones, chunks)),
             dma((zones, columns, chunks)), dma((zones, columns, chunks)),
             dma((zones, columns, chunks)), dma((zones, columns, chunks)),

time: 70.1 us -> 62.6 us (0.89); the launches traced: 69.9 us -> 61.6 us
  Pallas kernels: 67.8 us -> 59.5 us
    pallas_call x1, Pallas kernels: 67.8 us -> 59.5 us  [layer(): pl.pallas_call(functools.partial(layer_kernel, zones, group), out_shape=j...]
where the time goes in v2:
time: 62.6 us; the launch traced here: 61.6 us
  Pallas kernels  59.5 us (95%)
  local copies, waits for them, and re-layouts  2.09 us (3%)
    pallas_call x1, Pallas kernels, layer(): pl.pallas_call(functools.partial(layer_kernel, zones, group), out_shape=j...  59.5 us
    unnamed x1, local copies, waits for them, and re-layouts  2.09 us

profile of v2, /device:TPU:1, one launch (start us, length us, event | category | flops | bytes accessed | tf_op | source)
XLA Modules:
  0.0 61.6 jit_solution(14933446296114613691)
XLA Ops:
  0.0 59.5 %layer.1 = bf16[192,2048]{1,0:T(8,128)(2,1)} custom-call(bf16[192,2048]{1,0:T(8,128)(2,1)} %bitcast.10, f32[1,2048]{1,0:T(1,128)} %bitcast.14, bf16[512,128]{1,0:T(8,128)(2,1)} %wq_ref.1, bf16[32,512]{1,0:T(8,128)(2,1)} %bitcast.11, bf16[32,512]{1,0:T(8,128)(2,1)} %bitcast.12, f32[2,1536]{1,0:T(2,128)} %bitcast.13, f32[1,1024]{1,0:T(1,128)} %bitcast.15, ...), custom_call_target="tpu_custom_call" | custom-call | tf_op jit(solution)/shard_map/layer/pallas_call | solution.py:619
  59.5 2.1 %copy.10 = bf16[1,192,2048]{2,1,0:T(8,128)(2,1)} copy(bf16[1,192,2048]{2,1,0:T(8,128)(2,1)} %bitcast.9) | data formatting | bytes 1572864

commit v3 on v1

v3 whole, which is shorter than its diff:
```python
import functools
import math

import jax
import jax.numpy as jnp
from jax import lax
from jax.experimental import pallas as pl
from jax.experimental.pallas import tpu as pltpu
from jax.sharding import PartitionSpec as P

HEAD_DIM = 64
LOG2E = math.log2(math.e)
MESH = pl.DeviceIdType.MESH
VMEM_SPEC = pl.BlockSpec(memory_space=pltpu.VMEM)
ANY_SPEC = pl.BlockSpec(memory_space=pl.ANY)
f32, bf16 = jnp.float32, jnp.bfloat16


norm_eps = 1e-06
cores = 2
chunks = 2
halves = 2
aug = 16


def remote(source, target, send, recv, peer):
    copy = pltpu.make_async_remote_copy(
        src_ref=source, dst_ref=target, send_sem=send, recv_sem=recv,
        device_id=peer, device_id_type=MESH,
    )
    return copy


def layer_kernel(
    zones, group,
    x_hbm, in_gain_ref, wq_hbm, wk_ref, wv_ref, bias_ref, out_gain_ref, w_hbm, out_ref,
    x_ref, weights, x_far, normed, outbox, inbox, kvbox, k_aug, v_t, q_t, rest, total, tri,
    w_all, head, arrived, joined,
    own_sem, x_sem, wq_sem, send_z, recv_z, send_x, recv_x, send_c, recv_c, send_y, recv_y,
    send_m, recv_m, send_k, recv_k,
    send_wz, recv_wz, send_wa, recv_wa, send_wb, recv_wb, send_wc, recv_wc, send_h, recv_h,
):
    columns = lax.axis_size("dp") // cores
    sp, dp = lax.axis_index("sp"), lax.axis_index("dp")
    zone, place = sp // group, sp % group
    column, core = dp // cores, dp % cores
    rows, width = x_ref.shape
    size = zones * group
    span = group * rows
    pieces = columns * cores
    depth = width // pieces
    half = depth // 2
    cq = wq_hbm.shape[1]
    ck = wk_ref.shape[0]
    ck2 = 2 * ck
    fold = cq // ck2
    heads = bias_ref.shape[0]
    wide = heads * span
    some_rows = rows // halves
    deep = some_rows // fold
    piece_rows = weights.shape[2]
    part = piece_rows // chunks
    w_cols = w_hbm.shape[1]
    w_rows = w_hbm.shape[0]

    below, above = zone, zones - 1 - zone
    near = jnp.minimum(below, above)
    toward = jnp.where(below <= above, -1, 1)

    def source(n):
        if n == 0:
            return zone
        sign = toward if n % 2 == 1 else -toward
        offset = jnp.where(n <= 2 * near, sign * ((n + 1) // 2), -toward * (n - near))
        return zone + offset

    def at_zone(z):
        return {"sp": z * group + place}

    def at_column(j):
        return {"dp": lax.rem(column + j, columns) * cores + core}

    def at_place(g):
        return {"sp": zone * group + lax.rem(place + g, group)}

    def token_place(g):
        return lax.rem(place - g + group, group)

    partner = {"dp": column * cores + (1 - core)}

    barrier = pltpu.get_barrier_semaphore()
    peers = [
        {"sp": lax.rem(sp + k, size)} for k in range(1, size)
    ] + [at_column(j) for j in range(1, columns)] + [partner]
    for peer in peers:
        pl.semaphore_signal(barrier, inc=1, device_id=peer, device_id_type=MESH)

    wq_copy = pltpu.make_async_copy(wq_hbm, weights.at[zone, 0, pl.ds(0, depth), :], wq_sem)
    wq_copy.start()
    x_copy = pltpu.make_async_copy(x_hbm, x_ref, x_sem)
    x_copy.start()
    own_lanes = pl.ds(pl.multiple_of(dp * w_cols, w_cols), w_cols)
    own_weight = pltpu.make_async_copy(w_hbm, w_all.at[sp, :, own_lanes], own_sem)
    own_weight.start()

    pair = jnp.concatenate([wk_ref[...].astype(f32), wv_ref[...].astype(f32)], axis=0).T
    weights[zone, 0, depth:, :] = jnp.concatenate([pair[:half], pair[half:]], axis=1).astype(bf16)

    below_diag = lax.broadcasted_iota(jnp.int32, (rows, rows), 1) >= lax.broadcasted_iota(
        jnp.int32, (rows, rows), 0
    )
    tri[...] = jnp.where(below_diag, -1.0, 0.0).astype(bf16)
    mark_row = lax.broadcasted_iota(jnp.int32, (aug, wide), 0)
    mark_head = lax.broadcasted_iota(jnp.int32, (aug, wide), 1) // span
    marks = jnp.where(
        (mark_row >= 3 * mark_head) & (mark_row < 3 * mark_head + 3), 1.0, 0.0
    ).astype(bf16)
    for z in range(zones):
        q_t[z, 2 * HEAD_DIM :, :] = marks
    row_of = lax.broadcasted_iota(jnp.int32, (8, span), 0)
    for z in range(zones):
        tokens = slice(z * span, (z + 1) * span)
        terms = jnp.zeros((8, span), f32)
        for h in range(heads):
            value = bias_ref[h : h + 1, tokens] * LOG2E
            high = value.astype(bf16).astype(f32)
            middle = (value - high).astype(bf16).astype(f32)
            low = value - high - middle
            for i, term in enumerate((high, middle, low)):
                terms = jnp.where(row_of == 3 * h + i, term, terms)
        padded = jnp.concatenate([terms, jnp.zeros((120, span), f32)], axis=0)
        k_aug[tokens, 128:256] = padded.T.astype(bf16)

    wq_copy.wait()
    pl.semaphore_wait(barrier, len(peers))

    def piece(z, d):
        return weights.at[z, d]

    def some(z, d, c):
        return weights.at[z, d, pl.ds(c * part, part), :]

    def send_outward(n):
        z = source(n)
        for way, target in ((0, zone - 1), (1, zone + 1)):
            exists = (target >= 0) if way == 0 else (target < zones)
            if n > 0:
                exists = exists & ((z > zone) if way == 0 else (z < zone))
            yield way, at_zone(jnp.clip(target, 0, zones - 1)), exists

    def z_relay(n, c):
        z = source(n)
        for way, peer, exists in send_outward(n):
            copy = remote(some(z, 0, c), some(z, 0, c), send_z.at[n, way], recv_z.at[z, c], peer)

            @pl.when(exists)
            def _(copy=copy):
                copy.start()

    def z_sent(n):
        z = source(n)
        for way, peer, exists in send_outward(n):
            copy = remote(piece(z, 0), piece(z, 0), send_z.at[n, way], recv_z.at[z, 0], peer)

            @pl.when(exists)
            def _(copy=copy):
                copy.wait_send()

    def z_wait(n, c):
        z = source(n)
        remote(
            some(z, 0, c), some(z, 0, c), send_z.at[n, 0], recv_z.at[z, c], at_zone(zone)
        ).wait_recv()

    def x_spread(n, c):
        z = source(n)
        for j in range(1, columns):
            remote(
                some(z, 0, c), some(z, cores * j, c),
                send_x.at[j - 1], recv_x.at[n, j - 1], at_column(j),
            ).start()

    def to_partner(n, j):
        z = source(n)
        remote(
            piece(z, cores * j), piece(z, cores * j + 1), send_c.at[j], recv_c.at[n, j], partner
        ).start()

    def spread_columns(n):
        z = source(n)
        for j in range(1, columns):
            remote(
                piece(z, 0), piece(z, cores * j), send_x.at[j - 1], recv_x.at[n, j - 1], at_column(j)
            ).wait_recv()
            to_partner(n, j)

    def weights_sent():
        for n in range(zones):
            z_sent(n)
        for j in range(1, columns):
            remote(
                weights.at[:, 0], weights.at[:, 0], send_x.at[j - 1], recv_x.at[0, j - 1], partner
            ).wait_send()
        for j in range(columns):
            remote(
                weights.at[:, 0], weights.at[:, 0], send_c.at[j], recv_c.at[0, j], partner
            ).wait_send()

    def arrive(n):
        for c in range(chunks):
            if n > 0:
                z_wait(n, c)
            z_relay(n, c)
            x_spread(n, c)
        to_partner(n, 0)

    def normalize(rows_ref, g, first, count):
        step = 16

        def chunk(i, carry):
            here = pl.ds(pl.multiple_of(first + i * step, step), step)
            full = rows_ref[here, :].astype(f32)
            scale = lax.rsqrt(jnp.mean(full * full, axis=-1, keepdims=True) + norm_eps)
            for d in range(pieces):
                j, c = d // cores, d % cores
                index = lax.rem(column - j + columns, columns) * cores + (
                    core if c == 0 else 1 - core
                )
                for s in range(2):
                    lanes = pl.ds(pl.multiple_of(index * depth + s * half, half), half)
                    some = rows_ref[here, lanes].astype(f32) * scale * in_gain_ref[:, lanes]
                    normed[g, s, here, d * half : (d + 1) * half] = some.astype(bf16)
            return carry

        lax.fori_loop(0, count // step, chunk, 0)

    def project(n, g, parts=tuple(range(halves))):
        z = source(n)
        first, count = parts[0] * some_rows, len(parts) * some_rows
        key_weights = weights[z, :, depth : depth + half, :].reshape(pieces * half, cq)
        both = []
        for s in range(2):
            query_weights = weights[z, :, s * half : (s + 1) * half, :].reshape(pieces * half, cq)
            both.append(
                jnp.dot(
                    normed[g, s, first : first + count, :],
                    jnp.concatenate([query_weights, key_weights], axis=1),
                    preferred_element_type=f32,
                )
            )
        q = (both[0][:, :cq] + both[1][:, :cq]).astype(bf16)
        kv = both[0][:, cq : cq + ck2] + both[1][:, cq + ck2 : cq + 2 * ck2]
        tokens = token_place(g)
        for r in parts:
            mine = slice((r - parts[0]) * some_rows, (r - parts[0] + 1) * some_rows)
            q_part, kv_part = q[mine], kv[mine]
            kv_part = jnp.concatenate(
                [kv_part[i * deep : (i + 1) * deep] for i in range(fold)], axis=1
            ).astype(bf16)
            if n == 0:
                inbox[zone, tokens, r, :some_rows, :] = q_part
                inbox[zone, tokens, r, some_rows:, :] = kv_part
            else:
                outbox[n, g, r, :some_rows, :] = q_part
                outbox[n, g, r, some_rows:, :] = kv_part
        if n > 0:
            sent = pl.ds(parts[0], len(parts))
            remote(
                outbox.at[n, g, sent], inbox.at[zone, tokens, sent],
                send_m, recv_m.at[zone], at_zone(z),
            ).start()

    def share_keys(n):
        z = source(n)
        if n > 0:
            remote(inbox.at[z], inbox.at[z], send_m, recv_m.at[z], at_zone(zone)).wait_recv()
        for i in range(1, group):
            remote(
                inbox.at[z, :, :, pl.ds(some_rows, deep), :], kvbox.at[z, place],
                send_k.at[i - 1], recv_k.at[z, place], at_place(i),
            ).start()
        kvbox[z, place] = inbox[z, :, :, some_rows:, :]

    def keys_sent():
        remote(
            outbox.at[pl.ds(1, zones - 1)], outbox.at[pl.ds(1, zones - 1)],
            send_m, recv_m.at[zone], partner,
        ).wait_send()
        for i in range(1, group):
            every = inbox.at[:, :, :, pl.ds(some_rows, deep), :]
            remote(every, every, send_k.at[i - 1], recv_k.at[zone, place], partner).wait_send()

    def collect(n):
        z = source(n)
        for i in range(1, group):
            owner = token_place(i)
            remote(
                kvbox.at[z, owner], kvbox.at[z, owner],
                send_k.at[i - 1], recv_k.at[z, owner], at_place(i),
            ).wait_recv()
        for t in range(group):
            parts = []
            for p in range(group):
                packed = [kvbox[z, p, t, r].astype(f32) for r in range(halves)]
                parts.append(
                    jnp.concatenate(
                        [
                            packed[r][:, i * ck2 : (i + 1) * ck2]
                            for r in range(halves)
                            for i in range(fold)
                        ],
                        axis=0,
                    )
                )
            keys = [p[:, :ck] for p in parts]
            values = [p[:, ck:] for p in parts]
            target = pl.ds(pl.multiple_of((z * group + t) * rows, rows), rows)
            k_aug[target, 0:128] = jnp.concatenate(keys + keys, axis=1).astype(bf16)
            turned = jnp.concatenate(keys + values, axis=1).T
            v_t[z * group + t] = turned[HEAD_DIM:].astype(bf16)
        q = jnp.concatenate(
            [
                inbox[z, t, r, :some_rows, :].astype(f32)
                for t in range(group)
                for r in range(halves)
            ],
            axis=0,
        )
        turned = q.T * (LOG2E * HEAD_DIM**-0.5)
        high = turned.astype(bf16)
        low = (turned - high.astype(f32)).astype(bf16)
        for h in range(heads):
            lanes = slice(h * span, (h + 1) * span)
            own = slice(h * HEAD_DIM, (h + 1) * HEAD_DIM)
            q_t[z, :HEAD_DIM, lanes] = high[own]
            q_t[z, HEAD_DIM : 2 * HEAD_DIM, lanes] = low[own]

    def attend(qz, kz, diagonal):
        after = None if diagonal else rest[qz]
        acc = None if diagonal else total[qz]
        logits = {}
        for t in reversed(range(group)):
            window = pl.ds(pl.multiple_of((kz * group + t) * rows, rows), rows)
            logits[t] = jnp.dot(
                k_aug[window, : 2 * HEAD_DIM + aug], q_t[qz], preferred_element_type=f32
            )
        for t in reversed(range(group)):
            x = logits[t]
            soft = jnp.maximum(x, lax.log2(1.0 + lax.exp2(jnp.minimum(x, 126.0))))
            if diagonal:
                key = lax.broadcasted_iota(jnp.int32, (rows, wide), 0) + t * rows
                query = lax.rem(lax.broadcasted_iota(jnp.int32, (rows, wide), 1), span)
                strict = key < query
                soft = jnp.where(strict, soft, 0.0)
            kept = jnp.dot(tri[...], soft.astype(bf16), preferred_element_type=f32)
            power = x + kept
            if after is not None:
                power = power + after
            sticks = lax.exp2(power)
            if diagonal:
                sticks = jnp.where(strict, sticks, 0.0)
            more = jnp.dot(v_t[kz * group + t], sticks.astype(bf16), preferred_element_type=f32)
            acc = more if acc is None else acc + more
            after = kept[0:1, :] if after is None else after + kept[0:1, :]
        total[qz] = acc
        rest[qz] = after

    def send_head(s):
        return remote(
            head.at[pl.ds(s * rows, rows), :], arrived.at[sp], send_h, recv_h, {"sp": s}
        )

    def all_heads():
        others = pl.ds(0, (size - 1) * rows)
        return remote(head.at[others, :], head.at[others, :], send_h, recv_h, partner)

    def finish(qz):
        scaled = []
        for h in range(heads):
            some = total[qz, :, h * span : (h + 1) * span]
            scaled.append(
                some * lax.rsqrt(jnp.mean(some * some, axis=0, keepdims=True) + norm_eps)
            )
        lanes = pl.ds(pl.multiple_of(sp * cq, cq), cq) if cq % 128 == 0 else None
        gains = own_gain() if lanes is None else out_gain_ref[:, lanes]
        here = pl.ds(pl.multiple_of(qz * span, span), span)
        head[here, :] = (jnp.concatenate(scaled, axis=0).T * gains).astype(bf16)
        for t in range(group):
            s = qz * group + t

            @pl.when(s != sp)
            def _(s=s):
                send_head(s).start()

    def own_gain():
        both = out_gain_ref[:, pl.ds(pl.multiple_of(sp // 2 * 128, 128), 128)]
        return jnp.where(sp % 2 == 0, both[:, :cq], both[:, cq : 2 * cq])

    balanced = columns == group

    def lean_of(n):
        if not balanced:
            return 0
        return (core, 1, core, 1 - core)[n % 4]

    def weight(n, j, i):
        lean = lean_of(n)
        dx = j * (1 - lean) + i * lean
        dy = j * lean + i * (1 - lean)
        row = source(n) * group + lax.rem(place - dy + group, group)
        lane = lax.rem(column - dx + columns, columns) * cores + core
        return w_all.at[row, :, pl.ds(pl.multiple_of(lane * w_cols, w_cols), w_cols)]

    first_count = columns if not balanced else group
    second_count = group if not balanced else columns

    def at_first(n, j):
        lean = lean_of(n)
        return {
            "sp": zone * group + lax.rem(place + j * lean, group),
            "dp": lax.rem(column + j * (1 - lean), columns) * cores + core,
        }

    def at_second(n, i):
        lean = lean_of(n)
        return {
            "sp": zone * group + lax.rem(place + i * (1 - lean), group),
            "dp": lax.rem(column + i * lean, columns) * cores + core,
        }

    def w_core(n, j, i):
        remote(weight(n, j, i), weight(n, j, i), send_wc, recv_wc, partner).start()

    def w_second(n, j):
        for i in range(1, second_count):
            remote(
                weight(n, j, 0), weight(n, j, 0),
                send_wb.at[i - 1], recv_wb.at[n, j, i - 1], at_second(n, i),
            ).start()
        w_core(n, j, 0)

    def w_first(n):
        for j in range(1, first_count):
            remote(
                weight(n, 0, 0), weight(n, 0, 0),
                send_wa.at[j - 1], recv_wa.at[n, j - 1], at_first(n, j),
            ).start()
        w_second(n, 0)

    def w_sent():
        for n in range(zones):
            z = source(n)
            for way, peer, exists in send_outward(n):
                copy = remote(
                    weight(n, 0, 0), weight(n, 0, 0), send_wz.at[n, way], recv_wz.at[z], peer
                )

                @pl.when(exists)
                def _(copy=copy):
                    copy.wait_send()
        block = w_all.at[pl.ds(0, zones), :, pl.ds(0, w_cols)]
        for j in range(1, first_count):
            remote(block, block, send_wa.at[j - 1], recv_wa.at[0, j - 1], partner).wait_send()
        block = w_all.at[pl.ds(0, zones), :, pl.ds(0, first_count * w_cols)]
        for i in range(1, second_count):
            remote(block, block, send_wb.at[i - 1], recv_wb.at[0, 0, i - 1], partner).wait_send()

    def all_cores():
        block = w_all.at[:, :, pl.ds(0, columns * w_cols)]
        return remote(block, block, send_wc, recv_wc, partner)

    middle_zone = near > 0

    def wz_own(n):
        short = jnp.maximum(2 * near - 1, 0)
        for way, peer, exists in send_outward(0):
            fewer = above < below if way == 0 else below <= above
            last = jnp.where(fewer, short, zones - 1)
            copy = remote(
                weight(0, 0, 0), weight(0, 0, 0), send_wz.at[0, way], recv_wz.at[zone], peer
            )

            @pl.when(exists & (last == n))
            def _(copy=copy):
                copy.start()

    def wz_pass(n, now):
        z = source(n)

        @pl.when(now)
        def _():
            remote(
                weight(n, 0, 0), weight(n, 0, 0), send_wz.at[n, 0], recv_wz.at[z], at_zone(zone)
            ).wait_recv()
            for way, peer, exists in send_outward(n):
                copy = remote(
                    weight(n, 0, 0), weight(n, 0, 0), send_wz.at[n, way], recv_wz.at[z], peer
                )

                @pl.when(exists)
                def _(copy=copy):
                    copy.start()

    def w_first_event(n):
        for j in range(1, first_count):
            remote(
                weight(n, j, 0), weight(n, j, 0),
                send_wa.at[j - 1], recv_wa.at[n, j - 1], at_first(n, j),
            ).wait_recv()
            w_second(n, j)

    def w_second_event(n):
        for j in range(first_count):
            for i in range(1, second_count):
                remote(
                    weight(n, j, i), weight(n, j, i),
                    send_wb.at[i - 1], recv_wb.at[n, j, i - 1], at_second(n, i),
                ).wait_recv()
                w_core(n, j, i)

    def settle(n):
        for j in range(columns):
            z = source(n)
            remote(
                piece(z, cores * j), piece(z, cores * j + 1),
                send_c.at[j], recv_c.at[n, j], partner,
            ).wait_recv()

    def far(g, r):
        first = r * some_rows
        window = pl.ds(first, some_rows)
        return remote(
            x_ref.at[window, :], x_far.at[g - 1, window, :],
            send_y.at[g - 1, r], recv_y.at[g - 1, r], at_place(g),
        )

    def far_arrives(r):
        for g in range(1, group):
            far(g, r).wait_recv()
            normalize(x_far.at[g - 1], g, r * some_rows, some_rows)

    def far_project(n, parts):
        for g in range(1, group):
            project(n, g, parts)

    arrive(0)
    x_copy.wait()
    for r in range(halves):
        for g in range(1, group):
            far(g, r).start()
    own_weight.wait()
    wz_own(0)
    normalize(x_ref, 0, 0, rows)
    end_zone = jnp.logical_not(middle_zone)
    last = zones - 1
    for n in range(1, last):
        arrive(n)
        wz_own(n)
        if n == 1:
            spread_columns(0)
    settle(0)
    project(0, 0)

    @pl.when(middle_zone)
    def _():
        arrive(last)
        wz_own(last)
        wz_pass(1, middle_zone)

    for n in range(1, last):
        if n == last - 1:
            @pl.when(end_zone)
            def _():
                arrive(last)
                wz_own(last)

            w_first(0)
        spread_columns(n)
        if n == 1:
            far_arrives(0)
            far_project(0, (0,))
        settle(n)
        project(n, 0)
        far_project(n, (0,))
    far_arrives(1)
    for n in range(last):
        if n == 1:
            spread_columns(last)
        far_project(n, (1,))
    share_keys(0)
    settle(last)
    for g in range(group):
        project(last, g)
    wz_pass(1, end_zone)

    events = {}

    def at_slot(n, m, event, k):
        n = min(n, zones - 1)
        events.setdefault((n, min(m, n)), []).append((event, k))

    def late(n):
        wz_pass(n, end_zone)
        w_first(n)

    at_slot(1, 0, w_first_event, 1)
    for n in range(2, zones):
        at_slot(n - 1, 2 * n - 4, late, n)
        at_slot(n + 1, 4 * n - 8, w_first_event, n)
    at_slot(2, 0, w_second_event, 0)
    at_slot(2, 2, w_second_event, 1)

    for n in range(zones):
        if n + 1 < zones:
            share_keys(n + 1)
        if n == 0:
            for k in range(2, zones):
                wz_pass(k, middle_zone)
            w_first(1)
            w_first_event(0)
        collect(n)
        a = source(n)
        upward = a > zone if n > 0 else None
        attend(a, a, True)
        if n == 0:
            tiles = [(a, a)]
        else:
            tiles = [(a, a)] + [
                (jnp.where(upward, a, a + m), jnp.where(upward, a - m, a)) for m in range(1, n + 1)
            ]
        for m, (qz, kz) in enumerate(tiles):
            if m > 0:
                attend(qz, kz, False)

            @pl.when(kz == 0)
            def _(qz=qz):
                finish(qz)

            for event, k in events.get((n, m), []):
                event(k)
    for n in range(2, zones):
        w_second_event(n)
    mine = pltpu.make_async_copy(
        head.at[pl.ds(pl.multiple_of(sp * rows, rows), rows), :], arrived.at[sp], own_sem
    )
    mine.start()
    weights_sent()
    keys_sent()
    for r in range(halves):
        for g in range(1, group):
            far(g, r).wait_send()
    w_sent()
    mine.wait()
    all_heads().wait_recv()
    for s in range(size):
        joined[:, s * cq : (s + 1) * cq] = arrived[s]
    all_cores().wait_recv()
    strip = min(512, width)
    for i in range(width // strip):
        lanes = slice(i * strip, (i + 1) * strip)
        out_ref[:, lanes] = jnp.dot(
            joined[...], w_all[:, :, lanes].reshape(size * cq, strip), preferred_element_type=f32
        ).astype(bf16)
    all_cores().wait_send()
    all_heads().wait_send()


def layer(x, in_gain, wq, wk, wv, bias, out_gain, w_out, zones, group):
    rows, width = x.shape
    pieces = lax.axis_size("dp")
    columns = pieces // cores
    size = zones * group
    span = group * rows
    length = size * rows
    depth, cq = wq.shape
    ck2 = 2 * wk.shape[0]
    fold = cq // ck2
    heads = bias.shape[0]
    wide = heads * span
    some_rows = rows // halves
    deep = some_rows // fold
    dma = pltpu.SemaphoreType.DMA
    most = max(columns, group)
    return pl.pallas_call(
        functools.partial(layer_kernel, zones, group),
        out_shape=pltpu.VMEM((rows, width), bf16),
        in_specs=[ANY_SPEC, VMEM_SPEC, ANY_SPEC] + [VMEM_SPEC] * 4 + [ANY_SPEC],
        out_specs=VMEM_SPEC,
        scratch_shapes=[
            pltpu.VMEM((rows, width), bf16),
            pltpu.VMEM((zones, pieces, depth + depth // 2, cq), bf16),
            pltpu.VMEM((group - 1, rows, width), bf16),
            pltpu.VMEM((group, 2, rows, width // 2), bf16),
            pltpu.VMEM((zones, group, halves, some_rows + deep, cq), bf16),
            pltpu.VMEM((zones, group, halves, some_rows + deep, cq), bf16),
            pltpu.VMEM((zones, group, group, halves, deep, cq), bf16),
            pltpu.VMEM((length, 256), bf16),
            pltpu.VMEM((size, HEAD_DIM, rows), bf16),
            pltpu.VMEM((zones, 2 * HEAD_DIM + aug, wide), bf16),
            pltpu.VMEM((zones, 1, wide), f32),
            pltpu.VMEM((zones, HEAD_DIM, wide), f32),
            pltpu.VMEM((rows, rows), bf16),
            pltpu.VMEM((size, w_out.shape[0], width), bf16),
            pltpu.VMEM((length, cq), bf16),
            pltpu.VMEM((size, rows, cq), bf16),
            pltpu.VMEM((rows, size * cq), bf16),
            dma, dma, dma,
            dma((zones, 2)), dma((zones, chunks)),
            dma((columns - 1,)), dma((zones, columns - 1)),
            dma((columns,)), dma((zones, columns)),
            dma((group - 1, halves)), dma((group - 1, halves)),
            dma, dma((zones,)),
            dma((group - 1,)), dma((zones, group)),
            dma((zones, 2)), dma((zones,)),
            dma((most - 1,)), dma((zones, most - 1)),
            dma((most - 1,)), dma((zones, most, most - 1)),
            dma, dma,
            dma, dma,
        ],
        compiler_params=pltpu.CompilerParams(collective_id=0, has_side_effects=True),
        name="layer",
    )(x, in_gain, wq, wk, wv, bias, out_gain, w_out)


def body(inputs, in_gain, w_query, w_key, w_value, key_bias, out_gain, w_out):
    group = HEAD_DIM // w_key.shape[1]
    zones = lax.axis_size("sp") // group
    return layer(
        inputs[0], in_gain[None], w_query, w_key.T, w_value.T, key_bias[0].T,
        out_gain[None], w_out, zones, group,
    )[None]


def solution(mesh):
    placed = (
        P("dp", "sp", None),
        P(),
        P("dp", "sp"),
        P("dp", "sp"),
        P("dp", "sp"),
        P("dp", None, "sp"),
        P(),
        P("sp", "dp"),
    )
    return jax.shard_map(
        body, mesh=mesh, in_specs=placed, out_specs=P("dp", "sp", None), check_vma=False
    )
```

time: 70.1 us -> 60.4 us (0.86)
  Pallas kernels: 67.8 us -> 59.3 us
  local copies, waits for them, and re-layouts: 2.09 us -> 0.88 us
    pallas_call x1, Pallas kernels: 67.8 us -> 59.3 us  [layer(): pl.pallas_call(functools.partial(layer_kernel, zones, group), out_shape=p...]
    unnamed x1, local copies, waits for them, and re-layouts: 2.09 us -> 0.88 us
where the time goes in v3:
time: 60.4 us; the launch traced here: 60.2 us
  Pallas kernels  59.3 us (98%)
  local copies, waits for them, and re-layouts  0.88 us (1%)
    pallas_call x1, Pallas kernels, layer(): pl.pallas_call(functools.partial(layer_kernel, zones, group), out_shape=p...  59.3 us

profile of v3, /device:TPU:1, one launch (start us, length us, event | category | flops | bytes accessed | tf_op | source)
XLA Modules:
  0.0 60.2 jit_solution(7347554841558570060)
XLA Ops:
  0.0 59.3 %layer.1 = bf16[192,2048]{1,0:T(8,128)(2,1)S(1)} custom-call(bf16[192,2048]{1,0:T(8,128)(2,1)} %bitcast.10, f32[1,2048]{1,0:T(1,128)} %bitcast.14, bf16[512,128]{1,0:T(8,128)(2,1)} %wq_hbm.1, bf16[32,512]{1,0:T(8,128)(2,1)} %bitcast.11, bf16[32,512]{1,0:T(8,128)(2,1)} %bitcast.12, f32[2,1536]{1,0:T(2,128)} %bitcast.13, f32[1,1024]{1,0:T(1,128)} %bitcast.15, ...), custom_call_target="tpu_custom_call" | custom-call | tf_op jit(solution)/shard_map/layer/pallas_call | solution.py:684
  59.3 0.9 %copy.10 = bf16[1,192,2048]{2,1,0:T(8,128)(2,1)} copy(bf16[1,192,2048]{2,1,0:T(8,128)(2,1)S(1)} %bitcast.9) | data formatting | bytes 1572864

commit v4 on v3

--- a/solution.py
+++ b/solution.py
@@ -574,7 +574,6 @@
                 arrive(last)
                 wz_own(last)
 
-            w_first(0)
         spread_columns(n)
         if n == 1:
             far_arrives(0)
@@ -583,6 +582,7 @@
         project(n, 0)
         far_project(n, (0,))
     far_arrives(1)
+    w_first(0)
     for n in range(last):
         if n == 1:
             spread_columns(last)
@@ -603,21 +603,29 @@
         wz_pass(n, end_zone)
         w_first(n)
 
-    at_slot(1, 0, w_first_event, 1)
-    for n in range(2, zones):
-        at_slot(n - 1, 2 * n - 4, late, n)
-        at_slot(n + 1, 4 * n - 8, w_first_event, n)
-    at_slot(2, 0, w_second_event, 0)
+    at_slot(1, 1, w_first_event, 1)
+    for k in range(2, min(4, zones)):
+        at_slot(1, 1, share_keys, k)
+    at_slot(1, 1, late, 2)
+    at_slot(2, 1, w_second_event, 0)
+    at_slot(2, 2, late, 3)
     at_slot(2, 2, w_second_event, 1)
+    at_slot(3, 0, w_first_event, 2)
+    at_slot(3, 3, w_first_event, 3)
+    at_slot(3, 3, w_second_event, 2)
 
     for n in range(zones):
-        if n + 1 < zones:
-            share_keys(n + 1)
         if n == 0:
-            for k in range(2, zones):
+            wz_pass(2, middle_zone)
+            share_keys(1)
+            for k in range(3, zones):
                 wz_pass(k, middle_zone)
             w_first(1)
             w_first_event(0)
+        elif n > 3:
+            share_keys(n)
+            late(n)
+            w_first_event(n)
         collect(n)
         a = source(n)
         upward = a > zone if n > 0 else None
@@ -638,7 +646,7 @@
 
             for event, k in events.get((n, m), []):
                 event(k)
-    for n in range(2, zones):
+    for n in range(3, zones):
         w_second_event(n)
     mine = pltpu.make_async_copy(
         head.at[pl.ds(pl.multiple_of(sp * rows, rows), rows), :], arrived.at[sp], own_sem

time: 60.4 us -> 57.7 us (0.955)
  Pallas kernels: 59.3 us -> 56.6 us
    pallas_call x1, Pallas kernels: 59.3 us -> 56.6 us  [layer(): pl.pallas_call(functools.partial(layer_kernel, zones, group), out_shape=p...]
where the time goes in v4:
time: 57.7 us; the launch traced here: 57.5 us
  Pallas kernels  56.6 us (98%)
  local copies, waits for them, and re-layouts  0.88 us (2%)
    pallas_call x1, Pallas kernels, layer(): pl.pallas_call(functools.partial(layer_kernel, zones, group), out_shape=p...  56.6 us

profile of v4, /device:TPU:1, one launch (start us, length us, event | category | flops | bytes accessed | tf_op | source)
XLA Modules:
  0.0 57.5 jit_solution(5180257573469468559)
XLA Ops:
  0.0 56.6 %layer.1 = bf16[192,2048]{1,0:T(8,128)(2,1)S(1)} custom-call(bf16[192,2048]{1,0:T(8,128)(2,1)} %bitcast.10, f32[1,2048]{1,0:T(1,128)} %bitcast.14, bf16[512,128]{1,0:T(8,128)(2,1)} %wq_hbm.1, bf16[32,512]{1,0:T(8,128)(2,1)} %bitcast.11, bf16[32,512]{1,0:T(8,128)(2,1)} %bitcast.12, f32[2,1536]{1,0:T(2,128)} %bitcast.13, f32[1,1024]{1,0:T(1,128)} %bitcast.15, ...), custom_call_target="tpu_custom_call" | custom-call | tf_op jit(solution)/shard_map/layer/pallas_call | solution.py:692
  56.6 0.9 %copy.10 = bf16[1,192,2048]{2,1,0:T(8,128)(2,1)} copy(bf16[1,192,2048]{2,1,0:T(8,128)(2,1)S(1)} %bitcast.9) | data formatting | bytes 1572864

commit v5 on v4

--- a/solution.py
+++ b/solution.py
@@ -33,10 +33,10 @@
 
 def layer_kernel(
     zones, group,
-    x_hbm, in_gain_ref, wq_hbm, wk_ref, wv_ref, bias_ref, out_gain_ref, w_hbm, out_ref,
-    x_ref, weights, x_far, normed, outbox, inbox, kvbox, k_aug, v_t, q_t, rest, total, tri,
+    x_hbm, in_gain_hbm, wq_hbm, wk_hbm, wv_hbm, bias_hbm, out_gain_hbm, w_hbm, out_ref,
+    in_gain_ref, wk_ref, wv_ref, bias_ref, out_gain_ref, x_ref, weights, x_far, normed, outbox, inbox, kvbox, k_aug, v_t, q_t, rest, total, tri,
     w_all, head, arrived, joined,
-    own_sem, x_sem, wq_sem, send_z, recv_z, send_x, recv_x, send_c, recv_c, send_y, recv_y,
+    own_sem, x_sem, wq_sem, small_sem, send_z, recv_z, send_x, recv_x, send_c, recv_c, send_y, recv_y,
     send_m, recv_m, send_k, recv_k,
     send_wz, recv_wz, send_wa, recv_wa, send_wb, recv_wb, send_wc, recv_wc, send_h, recv_h,
 ):
@@ -51,10 +51,10 @@
     depth = width // pieces
     half = depth // 2
     cq = wq_hbm.shape[1]
-    ck = wk_ref.shape[0]
+    ck = wk_hbm.shape[0]
     ck2 = 2 * ck
     fold = cq // ck2
-    heads = bias_ref.shape[0]
+    heads = bias_hbm.shape[0]
     wide = heads * span
     some_rows = rows // halves
     deep = some_rows // fold
@@ -88,6 +88,16 @@
 
     partner = {"dp": column * cores + (1 - core)}
 
+    small = [
+        pltpu.make_async_copy(source, target, small_sem.at[i])
+        for i, (source, target) in enumerate(
+            (
+                (wk_hbm, wk_ref), (wv_hbm, wv_ref), (bias_hbm, bias_ref),
+                (in_gain_hbm, in_gain_ref), (out_gain_hbm, out_gain_ref),
+            )
+        )
+    ]
+
     barrier = pltpu.get_barrier_semaphore()
     peers = [
         {"sp": lax.rem(sp + k, size)} for k in range(1, size)
@@ -101,7 +111,11 @@
     x_copy.start()
     own_lanes = pl.ds(pl.multiple_of(dp * w_cols, w_cols), w_cols)
     own_weight = pltpu.make_async_copy(w_hbm, w_all.at[sp, :, own_lanes], own_sem)
+    for copy in small:
+        copy.start()
     own_weight.start()
+    for copy in small:
+        copy.wait()
 
     pair = jnp.concatenate([wk_ref[...].astype(f32), wv_ref[...].astype(f32)], axis=0).T
     weights[zone, 0, depth:, :] = jnp.concatenate([pair[:half], pair[half:]], axis=1).astype(bf16)
@@ -292,6 +306,22 @@
 
     def collect(n):
         z = source(n)
+        q = jnp.concatenate(
+            [
+                inbox[z, t, r, :some_rows, :].astype(f32)
+                for t in range(group)
+                for r in range(halves)
+            ],
+            axis=0,
+        )
+        turned = q.T * (LOG2E * HEAD_DIM**-0.5)
+        high = turned.astype(bf16)
+        low = (turned - high.astype(f32)).astype(bf16)
+        for h in range(heads):
+            lanes = slice(h * span, (h + 1) * span)
+            own = slice(h * HEAD_DIM, (h + 1) * HEAD_DIM)
+            q_t[z, :HEAD_DIM, lanes] = high[own]
+            q_t[z, HEAD_DIM : 2 * HEAD_DIM, lanes] = low[own]
         for i in range(1, group):
             owner = token_place(i)
             remote(
@@ -318,22 +348,6 @@
             k_aug[target, 0:128] = jnp.concatenate(keys + keys, axis=1).astype(bf16)
             turned = jnp.concatenate(keys + values, axis=1).T
             v_t[z * group + t] = turned[HEAD_DIM:].astype(bf16)
-        q = jnp.concatenate(
-            [
-                inbox[z, t, r, :some_rows, :].astype(f32)
-                for t in range(group)
-                for r in range(halves)
-            ],
-            axis=0,
-        )
-        turned = q.T * (LOG2E * HEAD_DIM**-0.5)
-        high = turned.astype(bf16)
-        low = (turned - high.astype(f32)).astype(bf16)
-        for h in range(heads):
-            lanes = slice(h * span, (h + 1) * span)
-            own = slice(h * HEAD_DIM, (h + 1) * HEAD_DIM)
-            q_t[z, :HEAD_DIM, lanes] = high[own]
-            q_t[z, HEAD_DIM : 2 * HEAD_DIM, lanes] = low[own]
 
     def attend(qz, kz, diagonal):
         after = None if diagonal else rest[qz]
@@ -553,6 +567,27 @@
     normalize(x_ref, 0, 0, rows)
     end_zone = jnp.logical_not(middle_zone)
     last = zones - 1
+    def late(n):
+        wz_pass(n, end_zone)
+        w_first(n)
+
+    def pass_on(n):
+        wz_pass(n, middle_zone)
+
+    plan = {
+        "far": [(w_first, 0)],
+        (1, 1): [(w_first_event, 1), (share_keys, 2), (share_keys, 3), (late, 2)],
+        "projected": [(pass_on, 2)],
+        "start": [(pass_on, 3), (late, 1), (w_first_event, 0)],
+        (2, 1): [(w_second_event, 0)],
+        (2, 2): [(late, 3), (w_second_event, 1), (w_first_event, 2)],
+        (3, 3): [(w_first_event, 3), (w_second_event, 2)],
+    }
+
+    def run(slot):
+        for event, k in plan.get(slot, ()):
+            event(k)
+
     for n in range(1, last):
         arrive(n)
         wz_own(n)
@@ -581,47 +616,24 @@
         settle(n)
         project(n, 0)
         far_project(n, (0,))
+        run(("early", n))
     far_arrives(1)
-    w_first(0)
+    run("far")
     for n in range(last):
         if n == 1:
             spread_columns(last)
         far_project(n, (1,))
     share_keys(0)
+    run("shared")
     settle(last)
     for g in range(group):
         project(last, g)
-    wz_pass(1, end_zone)
-
-    events = {}
-
-    def at_slot(n, m, event, k):
-        n = min(n, zones - 1)
-        events.setdefault((n, min(m, n)), []).append((event, k))
-
-    def late(n):
-        wz_pass(n, end_zone)
-        w_first(n)
-
-    at_slot(1, 1, w_first_event, 1)
-    for k in range(2, min(4, zones)):
-        at_slot(1, 1, share_keys, k)
-    at_slot(1, 1, late, 2)
-    at_slot(2, 1, w_second_event, 0)
-    at_slot(2, 2, late, 3)
-    at_slot(2, 2, w_second_event, 1)
-    at_slot(3, 0, w_first_event, 2)
-    at_slot(3, 3, w_first_event, 3)
-    at_slot(3, 3, w_second_event, 2)
+    run("projected")
 
     for n in range(zones):
         if n == 0:
-            wz_pass(2, middle_zone)
             share_keys(1)
-            for k in range(3, zones):
-                wz_pass(k, middle_zone)
-            w_first(1)
-            w_first_event(0)
+            run("start")
         elif n > 3:
             share_keys(n)
             late(n)
@@ -644,8 +656,7 @@
             def _(qz=qz):
                 finish(qz)
 
-            for event, k in events.get((n, m), []):
-                event(k)
+            run((n, m))
     for n in range(3, zones):
         w_second_event(n)
     mine = pltpu.make_async_copy(
@@ -662,13 +673,17 @@
     all_heads().wait_recv()
     for s in range(size):
         joined[:, s * cq : (s + 1) * cq] = arrived[s]
+    def multiply(c):
+        for j in range(columns):
+            lanes = pl.ds(pl.multiple_of((j * cores + c) * w_cols, w_cols), w_cols)
+            out_ref[:, lanes] = jnp.dot(
+                joined[...], w_all[:, :, lanes].reshape(size * cq, w_cols),
+                preferred_element_type=f32,
+            ).astype(bf16)
+
+    multiply(core)
     all_cores().wait_recv()
-    strip = min(512, width)
-    for i in range(width // strip):
-        lanes = slice(i * strip, (i + 1) * strip)
-        out_ref[:, lanes] = jnp.dot(
-            joined[...], w_all[:, :, lanes].reshape(size * cq, strip), preferred_element_type=f32
-        ).astype(bf16)
+    multiply(1 - core)
     all_cores().wait_send()
     all_heads().wait_send()
 
@@ -692,9 +707,14 @@
     return pl.pallas_call(
         functools.partial(layer_kernel, zones, group),
         out_shape=pltpu.VMEM((rows, width), bf16),
-        in_specs=[ANY_SPEC, VMEM_SPEC, ANY_SPEC] + [VMEM_SPEC] * 4 + [ANY_SPEC],
+        in_specs=[ANY_SPEC] * 8,
         out_specs=VMEM_SPEC,
         scratch_shapes=[
+            pltpu.VMEM(in_gain.shape, f32),
+            pltpu.VMEM(wk.shape, bf16),
+            pltpu.VMEM(wv.shape, bf16),
+            pltpu.VMEM(bias.shape, f32),
+            pltpu.VMEM(out_gain.shape, f32),
             pltpu.VMEM((rows, width), bf16),
             pltpu.VMEM((zones, pieces, depth + depth // 2, cq), bf16),
             pltpu.VMEM((group - 1, rows, width), bf16),
@@ -712,7 +732,7 @@
             pltpu.VMEM((length, cq), bf16),
             pltpu.VMEM((size, rows, cq), bf16),
             pltpu.VMEM((rows, size * cq), bf16),
-            dma, dma, dma,
+            dma, dma, dma, dma((5,)),
             dma((zones, 2)), dma((zones, chunks)),
             dma((columns - 1,)), dma((zones, columns - 1)),
             dma((columns,)), dma((zones, columns)),

time: 57.7 us -> 56 us (0.971)
  Pallas kernels: 56.6 us -> 54.9 us
    pallas_call x1, Pallas kernels: 56.6 us -> 54.9 us  [layer(): pl.pallas_call(functools.partial(layer_kernel, zones, group), out_shape=p...]
where the time goes in v5:
time: 56 us; the launch traced here: 55.8 us
  Pallas kernels  54.9 us (98%)
  local copies, waits for them, and re-layouts  0.88 us (2%)
    pallas_call x1, Pallas kernels, layer(): pl.pallas_call(functools.partial(layer_kernel, zones, group), out_shape=p...  54.9 us

profile of v5, /device:TPU:1, one launch (start us, length us, event | category | flops | bytes accessed | tf_op | source)
XLA Modules:
  0.0 55.8 jit_solution(5736592870566081767)
XLA Ops:
  0.0 54.9 %layer.1 = bf16[192,2048]{1,0:T(8,128)(2,1)S(1)} custom-call(bf16[192,2048]{1,0:T(8,128)(2,1)} %bitcast.10, f32[1,2048]{1,0:T(1,128)} %bitcast.14, bf16[512,128]{1,0:T(8,128)(2,1)} %wq_hbm.1, bf16[32,512]{1,0:T(8,128)(2,1)} %bitcast.11, bf16[32,512]{1,0:T(8,128)(2,1)} %bitcast.12, f32[2,1536]{1,0:T(2,128)} %bitcast.13, f32[1,1024]{1,0:T(1,128)} %bitcast.15, ...), custom_call_target="tpu_custom_call" | custom-call | tf_op jit(solution)/shard_map/layer/pallas_call | solution.py:707
  54.9 0.9 %copy.10 = bf16[1,192,2048]{2,1,0:T(8,128)(2,1)} copy(bf16[1,192,2048]{2,1,0:T(8,128)(2,1)S(1)} %bitcast.9) | data formatting | bytes 1572864

commit v6 on v5

--- a/solution.py
+++ b/solution.py
@@ -349,6 +349,11 @@
             turned = jnp.concatenate(keys + values, axis=1).T
             v_t[z * group + t] = turned[HEAD_DIM:].astype(bf16)
 
+    def strict(t):
+        key = lax.broadcasted_iota(jnp.int32, (rows, wide), 0) + t * rows
+        query = lax.rem(lax.broadcasted_iota(jnp.int32, (rows, wide), 1), span)
+        return key < query
+
     def attend(qz, kz, diagonal):
         after = None if diagonal else rest[qz]
         acc = None if diagonal else total[qz]
@@ -358,24 +363,23 @@
             logits[t] = jnp.dot(
                 k_aug[window, : 2 * HEAD_DIM + aug], q_t[qz], preferred_element_type=f32
             )
+        kept = {}
         for t in reversed(range(group)):
-            x = logits[t]
-            soft = jnp.maximum(x, lax.log2(1.0 + lax.exp2(jnp.minimum(x, 126.0))))
+            soft = logits[t]
+            soft = jnp.maximum(soft, lax.log2(1.0 + lax.exp2(jnp.minimum(soft, 126.0))))
             if diagonal:
-                key = lax.broadcasted_iota(jnp.int32, (rows, wide), 0) + t * rows
-                query = lax.rem(lax.broadcasted_iota(jnp.int32, (rows, wide), 1), span)
-                strict = key < query
-                soft = jnp.where(strict, soft, 0.0)
-            kept = jnp.dot(tri[...], soft.astype(bf16), preferred_element_type=f32)
-            power = x + kept
+                soft = jnp.where(strict(t), soft, 0.0)
+            kept[t] = jnp.dot(tri[...], soft.astype(bf16), preferred_element_type=f32)
+        for t in reversed(range(group)):
+            power = logits[t] + kept[t]
             if after is not None:
                 power = power + after
             sticks = lax.exp2(power)
             if diagonal:
-                sticks = jnp.where(strict, sticks, 0.0)
+                sticks = jnp.where(strict(t), sticks, 0.0)
             more = jnp.dot(v_t[kz * group + t], sticks.astype(bf16), preferred_element_type=f32)
             acc = more if acc is None else acc + more
-            after = kept[0:1, :] if after is None else after + kept[0:1, :]
+            after = kept[t][0:1, :] if after is None else after + kept[t][0:1, :]
         total[qz] = acc
         rest[qz] = after
 

time: 56 us -> 56 us (level)
  no operation moved by 1% of the time
where the time goes in v6:
time: 56 us; the launch traced here: 55.9 us
  Pallas kernels  55 us (98%)
  local copies, waits for them, and re-layouts  0.88 us (2%)
    pallas_call x1, Pallas kernels, layer(): pl.pallas_call(functools.partial(layer_kernel, zones, group), out_shape=p...  55 us

profile of v6, /device:TPU:1, one launch (start us, length us, event | category | flops | bytes accessed | tf_op | source)
XLA Modules:
  0.0 55.9 jit_solution(13409786721390894949)
XLA Ops:
  0.0 55.0 %layer.1 = bf16[192,2048]{1,0:T(8,128)(2,1)S(1)} custom-call(bf16[192,2048]{1,0:T(8,128)(2,1)} %bitcast.10, f32[1,2048]{1,0:T(1,128)} %bitcast.14, bf16[512,128]{1,0:T(8,128)(2,1)} %wq_hbm.1, bf16[32,512]{1,0:T(8,128)(2,1)} %bitcast.11, bf16[32,512]{1,0:T(8,128)(2,1)} %bitcast.12, f32[2,1536]{1,0:T(2,128)} %bitcast.13, f32[1,1024]{1,0:T(1,128)} %bitcast.15, ...), custom_call_target="tpu_custom_call" | custom-call | tf_op jit(solution)/shard_map/layer/pallas_call | solution.py:711
  55.0 0.9 %copy.10 = bf16[1,192,2048]{2,1,0:T(8,128)(2,1)} copy(bf16[1,192,2048]{2,1,0:T(8,128)(2,1)S(1)} %bitcast.9) | data formatting | bytes 1572864
